TPU v7x, 128 devices: a whole 4x4x4 slice. The times are simulated.
128 devices in a mesh: sp: 16 (over z, y), tp: 8 (over x, core).
Axes of the slice: x: 4, y: 4, z: 4, core: 2. Of those that a mesh axis runs over, the one named last changes fastest.
Arguments:
- arriving_hidden_state: bfloat16 [16384, 2048], P(('sp', 'tp')), may hold values from -6 to 6
- former_request_vectors: bfloat16 [16384, 1024], P('sp', 'tp'), may hold values from -6 to 6
- former_match_vectors: bfloat16 [16384, 1024], P('sp', 'tp'), may hold values from -6 to 6
- latter_request_vectors: bfloat16 [16384, 512], P('sp', 'tp'), may hold values from -6 to 6
- latter_match_vectors: bfloat16 [16384, 512], P('sp', 'tp'), may hold values from -6 to 6
- stored_vectors_both: bfloat16 [16384, 2, 1024], P('sp', None, 'tp'), may hold values from -6 to 6
- closing_valve_operands: bfloat16 [16384, 2, 1024], P('sp', None, 'tp'), may hold values from -6 to 6
- update_level_before_squash: bfloat16 [2, 8, 16384], P(None, 'tp', 'sp'), may hold values from -4 to -3
- fading_data_input: float32 [2, 8, 16384], P(None, 'tp', 'sp'), may hold values from -5.5 to 5.5
- sparse_fading_boost: float32 [2, 8, 16384], P(None, 'tp', 'sp'), may hold values from -2 to 0, as said below
- unitwise_fading_loglevel: float32 [2, 8], P(None, 'tp'), as said below
- fading_constant_term: float32 [2, 8], P(None, 'tp'), may hold values from -1 to 1
- unitwise_normalizer_coef: float32 [128], replicated, may hold values from 0.1 to 1.9
- emission_map_weights: bfloat16 [2048, 2048], replicated, may hold values from -0.125 to 0.125
- channel_normalizer_coef: float32 [2048], replicated, may hold values from 0.1 to 1.9
- switching_channel_map: bfloat16 [2048, 6144], P('sp', 'tp'), may hold values from -0.125 to 0.125
- broadening_channel_map: bfloat16 [2048, 6144], P('sp', 'tp'), may hold values from -0.125 to 0.125
- timewise_convolve_tapvalues: bfloat16 [3, 2, 6144], P(None, None, 'tp'), may hold values from -3.5 to 3.5
- narrowing_map_weights_in: bfloat16 [2048, 6144], P('sp', 'tp'), may hold values from -0.078125 to 0.078125
Outputs:
- mixed: bfloat16 [16384, 2048], P(('sp', 'tp'))
Inputs may be any that keep to these rules, and one draw needn't show every extreme that they name: `unitwise_fading_loglevel`: each entry is the logarithm of a per-position rate between 0.2 / 16384 and 2 / 64. `sparse_fading_boost`: zero except at three or fewer positions of the sequence.
All inputs are finite; a program needn't handle non-finite values.
Results may differ from a plain program's by a relative error of at most 0.015.
Values may be sent and summed in bfloat16 or wider, within the bound.
A program may use at most 128 MiB of HBM per device.

v0:
```python
import jax
import jax.numpy as jnp
from jax import lax
from jax.experimental import pallas as pl
from jax.experimental.pallas import tpu as pltpu
from jax.sharding import Mesh
from jax.sharding import PartitionSpec as P

TAPS = 3
SP = ("sp_0", "sp_1")
SP_TP = ("sp_0", "sp_1", "tp")

BLK = 128
NBLK = 8
EPSILON = 1e-06
F32 = jnp.float32
BF16 = jnp.bfloat16


def mm(a, b):
    return jnp.dot(a.astype(BF16), b.astype(BF16), preferred_element_type=F32)


def mm_nt(a, b):
    return lax.dot_general(
        a.astype(BF16), b.astype(BF16), (((1,), (1,)), ((), ())), preferred_element_type=F32
    )


def normed_rows(x, scale):
    return x * (lax.rsqrt(jnp.sum(x * x, axis=-1, keepdims=True) + EPSILON) * scale)


def fold_blocks(row):
    return jnp.concatenate([row[:, i * BLK : (i + 1) * BLK] for i in range(NBLK)], axis=0)


def gate_rows(upd, fade, boost, loglevel, bias):
    beta = 1.0 / (1.0 + jnp.exp(-fold_blocks(upd.astype(F32))))
    pre = fold_blocks(fade) + bias
    soft = jnp.maximum(pre, 0.0) + jnp.log1p(jnp.exp(-jnp.abs(pre)))
    rate = jnp.exp(jnp.full((NBLK, BLK), loglevel, F32))
    cum = fold_blocks(boost) - rate * soft
    lane = lax.broadcasted_iota(jnp.int32, (NBLK, BLK), 1)
    step = 1
    while step < BLK:
        cum = cum + jnp.where(lane >= step, pltpu.roll(cum, step, 1), 0.0)
        step *= 2
    return beta, cum


def block_inputs(q, k, v, cum_row, beta_row):
    dk = q.shape[-1]
    c_j = jnp.broadcast_to(cum_row, (BLK, BLK))
    c_i = c_j.T
    b_i = jnp.broadcast_to(beta_row, (BLK, BLK)).T
    row = lax.broadcasted_iota(jnp.int32, (BLK, BLK), 0)
    col = lax.broadcasted_iota(jnp.int32, (BLK, BLK), 1)
    decay = jnp.exp(jnp.where(row >= col, c_i - c_j, -1e30))
    e_i = jnp.exp(c_i)
    c_last = jnp.broadcast_to(cum_row[:, BLK - 1 :], (1, BLK))
    qn = normed_rows(q.astype(F32), dk**-0.5)
    kn = normed_rows(k.astype(F32), 1.0)
    kb = kn.astype(BF16)
    both = mm_nt(jnp.concatenate([kb, qn.astype(BF16)], axis=0), kb)
    lower = jnp.where(row > col, -(b_i * both[:BLK] * decay), 0.0)
    intra = (both[BLK:] * decay).astype(BF16)
    right = jnp.concatenate([v.astype(F32) * b_i, kn * (b_i * e_i)[:, :dk]], axis=1)
    tail = kn * jnp.exp(c_last - c_i)[:, :dk]
    return dict(
        lower=lower,
        intra=intra,
        right=right,
        tail=tail.T.astype(BF16),
        query=qn * e_i[:, :dk],
        keep=jnp.exp(c_last),
    )


def inverses(lowers):
    powers = [n.astype(BF16) for n in lowers]
    extra = list(lowers)
    power = [mm(p, p) for p in powers]
    for level in range(1, 7):
        pb = [p.astype(BF16) for p in power]
        if level < 6:
            wide = [
                mm(p, jnp.concatenate([e.astype(BF16), p], axis=1)) for p, e in zip(pb, extra)
            ]
            extra = [e + p + w[:, :BLK] for e, p, w in zip(extra, power, wide)]
            power = [w[:, BLK:] for w in wide]
        else:
            extra = [e + p + mm(q, e) for e, p, q in zip(extra, power, pb)]
    return extra


def local_kernel(
    q1, k1, q2, k2, vals, upd, fade, boost, level, bias,
    r1, r2, o1, o2, pay,
    beta_s, cum_s, keep_s, qd1, qd2, loc1, loc2, add1, add2,
):
    for h in range(2):
        beta, cum = gate_rows(upd[h], fade[h], boost[h], level[h, 0], bias[h, 0])
        beta_s[h * NBLK : (h + 1) * NBLK, :] = beta
        cum_s[h * NBLK : (h + 1) * NBLK, :] = cum

    def parts(it, carry):
        todo = [(h, 2 * it + j) for j in range(2) for h in range(2)]
        ins = []
        for h, n in todo:
            rows = pl.ds(pl.multiple_of(n * BLK, BLK), BLK)
            q, k = (q1, k1) if h == 0 else (q2, k2)
            ins.append(
                block_inputs(
                    q[rows, :],
                    k[rows, :],
                    vals[rows, h * BLK : (h + 1) * BLK],
                    cum_s[pl.ds(h * NBLK + n, 1), :],
                    beta_s[pl.ds(h * NBLK + n, 1), :],
                )
            )
        extra = inverses([i["lower"] for i in ins])
        for (h, n), i, e in zip(todo, ins, extra):
            dk = (128, 64)[h]
            solved = (i["right"] + mm(e, i["right"])).astype(BF16)
            made = mm(jnp.concatenate([i["intra"], i["tail"]], axis=0), solved)
            qd, loc, add = ((qd1, loc1, add1), (qd2, loc2, add2))[h]
            qd[n, :BLK, :] = (i["query"] - made[:BLK, BLK:]).astype(BF16)
            qd[n, BLK:, :] = (-made[BLK:, BLK:]).astype(BF16)
            loc[n] = made[:BLK, :BLK]
            add[n] = made[BLK:, :BLK]
            keep_s[pl.ds(h * NBLK + n, 1), :] = i["keep"]
        return carry

    lax.fori_loop(0, NBLK // 2, parts, 0)

    def eye(dk):
        return (
            lax.broadcasted_iota(jnp.int32, (dk, dk), 0)
            == lax.broadcasted_iota(jnp.int32, (dk, dk), 1)
        ).astype(F32)

    def chain(n, carry):
        rows = pl.ds(pl.multiple_of(n * BLK, BLK), BLK)
        out = []
        for h, (state, total) in enumerate(carry):
            dk = (128, 64)[h]
            qd, loc, add = ((qd1, loc1, add1), (qd2, loc2, add2))[h]
            r, o = ((r1, o1), (r2, o2))[h]
            made = mm(qd[n], state)
            o[rows, :] = loc[n] + made[:BLK, :BLK]
            r[rows, :] = made[:BLK, BLK:].astype(BF16)
            keep = keep_s[pl.ds(h * NBLK + n, 1), :]
            moved = made[BLK:]
            new_a = state[:, :BLK] * keep + moved[:, :BLK] + add[n]
            new_p = state[:, BLK:] * keep[:, :dk] + moved[:, BLK:]
            out.append((jnp.concatenate([new_a, new_p], axis=1), total * keep))
        return tuple(out)

    start = tuple(
        (jnp.concatenate([jnp.zeros((dk, BLK), F32), eye(dk)], axis=1), jnp.ones((1, BLK), F32))
        for dk in (128, 64)
    )
    (s1, g1), (s2, g2) = lax.fori_loop(0, NBLK, chain, start)
    pay[0:128, :] = (s1[:, BLK:] - eye(128) * g1).astype(BF16)
    pay[128:256, :] = s1[:, :BLK].astype(BF16)
    pay[256:320, :] = s2[:, :BLK].astype(BF16)
    row = lax.broadcasted_iota(jnp.int32, (64, 64), 0)
    hi1, hi2 = g1.astype(BF16).astype(F32), g2.astype(BF16).astype(F32)
    scal = jnp.where(row == 0, hi1[:, :64], 0.0)
    scal = scal + jnp.where(row == 1, (g1 - hi1)[:, :64], 0.0)
    scal = scal + jnp.where(row == 2, hi2[:, :64], 0.0)
    scal = scal + jnp.where(row == 3, (g2 - hi2)[:, :64], 0.0)
    d2 = s2[:, BLK:] - eye(64) * g2[:, :64]
    pay[320:384, :] = jnp.concatenate([d2, scal], axis=1).astype(BF16)


def local_recurrence(q1, k1, q2, k2, vals, upd, fade, boost, level, bias):
    vm = pl.BlockSpec(memory_space=pltpu.VMEM)
    sm = pl.BlockSpec(memory_space=pltpu.SMEM)
    return pl.pallas_call(
        local_kernel,
        out_shape=(
            jax.ShapeDtypeStruct((1024, 128), BF16),
            jax.ShapeDtypeStruct((1024, 64), BF16),
            jax.ShapeDtypeStruct((1024, 128), F32),
            jax.ShapeDtypeStruct((1024, 128), F32),
            jax.ShapeDtypeStruct((384, 128), BF16),
        ),
        in_specs=[vm] * 8 + [sm] * 2,
        out_specs=[vm] * 5,
        scratch_shapes=[
            pltpu.VMEM((2 * NBLK, BLK), F32),
            pltpu.VMEM((2 * NBLK, BLK), F32),
            pltpu.VMEM((2 * NBLK, BLK), F32),
            pltpu.VMEM((NBLK, 256, 128), BF16),
            pltpu.VMEM((NBLK, 192, 64), BF16),
            pltpu.VMEM((NBLK, BLK, BLK), F32),
            pltpu.VMEM((NBLK, BLK, BLK), F32),
            pltpu.VMEM((NBLK, 128, BLK), F32),
            pltpu.VMEM((NBLK, 64, BLK), F32),
        ],
        cost_estimate=pl.CostEstimate(
            flops=2_000_000_000, bytes_accessed=4_000_000, transcendentals=1_000_000
        ),
    )(q1, k1, q2, k2, vals, upd, fade, boost, level, bias)


def split_pay(pay):
    p = pay.astype(F32)
    g1 = p[320, 64] + p[321, 64]
    g2 = p[322, 64] + p[323, 64]
    return (p[:128], p[128:256], g1), (p[320:, :64], p[256:320], g2)


def join_pay(one, two):
    (d1, a1, g1), (d2, a2, g2) = one, two
    hi1, hi2 = lax.reduce_precision(g1, 8, 7), lax.reduce_precision(g2, 8, 7)
    scal = jnp.stack([hi1, g1 - hi1, hi2, g2 - hi2])
    scal = jnp.pad(jnp.broadcast_to(scal[:, None], (4, 64)), ((0, 60), (0, 0)))
    low = jnp.concatenate([d2, scal], axis=1)
    return jnp.concatenate([d1, a1, a2, low], axis=0).astype(BF16)


def after(earlier, later):
    d0, a0, g0 = earlier
    d1, a1, g1 = later
    return (g1 * d0 + g0 * d1 + mm(d1, d0), g1 * a0 + a1 + mm(d1, a0), g0 * g1)


def applied(later, state):
    d, a, g = later
    return g * state + a + mm(d, state)


def incoming_states(pay):
    y, z = lax.axis_index("sp_1"), lax.axis_index("sp_0")
    row = lax.all_gather(pay, "sp_1")
    members = [split_pay(row[i]) for i in range(4)]
    whole = members[0]
    for m in members[1:]:
        whole = tuple(after(e, l) for e, l in zip(whole, m))
    rows = lax.all_gather(join_pay(*whole), "sp_0")
    states = [jnp.zeros((128, 128), F32), jnp.zeros((64, 128), F32)]
    for i in range(3):
        states = [
            jnp.where(i < z, applied(m, s), s) for m, s in zip(split_pay(rows[i]), states)
        ]
    for i in range(3):
        states = [jnp.where(i < y, applied(m, s), s) for m, s in zip(members[i], states)]
    return states


def finished_head(local, reads, state, gate_cols, coef):
    out = local + mm(reads, state)
    scaled = out * lax.rsqrt(jnp.mean(out * out, axis=-1, keepdims=True) + EPSILON) * coef
    return (scaled * jax.nn.silu(gate_cols.astype(F32))).astype(BF16)


def from_behind(value, axis, steps):
    count = lax.axis_size(axis)
    leading, last = (max(0, -steps), min(count, count - steps))
    return lax.ppermute(value, axis, [(source, source + steps) for source in range(leading, last)])


def split_up(shard, dim, size):
    lengths = shard.shape
    tiles = shard.reshape(*lengths[:dim], size, lengths[dim] // size, *lengths[dim + 1 :])
    return jnp.moveaxis(tiles, dim, 0)


def summed_on_arrival(shard, axis, dim):
    tiles = split_up(shard, dim, lax.axis_size(axis))
    arrived = lax.all_to_all(tiles, axis, split_axis=0, concat_axis=0, tiled=True)
    return arrived.astype(jnp.float32).sum(axis=0)


def causal_taps(edge_rows, low_rows, taps_col):
    padded = jnp.concatenate([edge_rows, low_rows], axis=0)
    length = low_rows.shape[0]
    total = taps_col[0] * padded[0:length]
    for tap_index in range(1, TAPS):
        total = total + taps_col[tap_index] * padded[tap_index : tap_index + length]
    return total


def per_device(
    arriving_hidden_state,
    former_request_vectors,
    former_match_vectors,
    latter_request_vectors,
    latter_match_vectors,
    stored_vectors_both,
    closing_valve_operands,
    update_level_before_squash,
    fading_data_input,
    sparse_fading_boost,
    unitwise_fading_loglevel,
    fading_constant_term,
    unitwise_normalizer_coef,
    emission_map_weights,
    channel_normalizer_coef,
    switching_channel_map,
    broadening_channel_map,
    timewise_convolve_tapvalues,
    narrowing_map_weights_in,
):
    gathered = lax.all_gather(
        jnp.concatenate(
            [switching_channel_map, broadening_channel_map, narrowing_map_weights_in], axis=1
        ),
        SP,
        axis=0,
        tiled=True,
    )
    vals = stored_vectors_both.reshape(-1, 256)
    r1, r2, o1, o2, pay = local_recurrence(
        former_request_vectors,
        former_match_vectors,
        latter_request_vectors,
        latter_match_vectors,
        vals,
        update_level_before_squash,
        fading_data_input,
        sparse_fading_boost,
        unitwise_fading_loglevel,
        fading_constant_term,
    )
    s1, s2 = incoming_states(pay)
    linear_attend = jnp.stack(
        [
            finished_head(o1, r1, s1, closing_valve_operands[:, 0], unitwise_normalizer_coef),
            finished_head(o2, r2, s2, closing_valve_operands[:, 1], unitwise_normalizer_coef),
        ],
        axis=1,
    )
    arrived = lax.all_to_all(linear_attend, "tp", split_axis=0, concat_axis=2, tiled=True)
    row_count = arrived.shape[0]
    skip_stream = arriving_hidden_state.astype(jnp.float32) + jnp.dot(
        arrived.reshape(row_count, -1), emission_map_weights, preferred_element_type=jnp.float32
    )
    normed = (
        skip_stream
        * lax.rsqrt(jnp.mean(skip_stream * skip_stream, axis=-1, keepdims=True) + EPSILON)
        * channel_normalizer_coef
    ).astype(jnp.bfloat16)
    features = lax.all_gather(normed, "tp", axis=0, tiled=True)
    gate_full = jnp.dot(features, gathered[:, :768], preferred_element_type=jnp.float32)
    up_full = jnp.dot(features, gathered[:, 768:1536], preferred_element_type=jnp.float32)
    gate_low = gate_full.astype(jnp.bfloat16)
    up_low = up_full.astype(jnp.bfloat16)
    edge_gate, edge_up = from_behind((gate_low[-(TAPS - 1) :], up_low[-(TAPS - 1) :]), SP, 1)
    taps = timewise_convolve_tapvalues.astype(jnp.float32)
    gate_conv = causal_taps(edge_gate, gate_low, taps[:, 0])
    up_conv = causal_taps(edge_up, up_low, taps[:, 1])
    hidden = (jax.nn.silu(gate_conv) * up_conv).astype(jnp.bfloat16)
    down_sum = summed_on_arrival(
        lax.dot_general(
            hidden, gathered[:, 1536:], (((1,), (1,)), ((), ())), preferred_element_type=jnp.float32
        ).astype(jnp.bfloat16),
        "tp",
        0,
    )
    return (skip_stream + down_sum).astype(jnp.bfloat16)


def solution(mesh):
    torus = Mesh(mesh.devices.reshape(4, 4, mesh.shape["tp"]), ("sp_0", "sp_1", "tp"))
    return jax.shard_map(
        per_device,
        mesh=torus,
        in_specs=(
            P(SP_TP, None),
            P(SP, "tp"),
            P(SP, "tp"),
            P(SP, "tp"),
            P(SP, "tp"),
            P(SP, None, "tp"),
            P(SP, None, "tp"),
            P(None, "tp", SP),
            P(None, "tp", SP),
            P(None, "tp", SP),
            P(None, "tp"),
            P(None, "tp"),
            P(),
            P(),
            P(),
            P(SP, "tp"),
            P(SP, "tp"),
            P(None, None, "tp"),
            P(SP, "tp"),
        ),
        out_specs=P(SP_TP, None),
        check_vma=False,
    )
```

profile of v0, /device:TPU:1, one launch (start us, length us, event | category | flops | bytes accessed | tf_op | source)
XLA Modules:
  0.0 309.8 jit_solution(6351642623937099379)
XLA Ops:
  6.5 1.2 copy.52.level
  7.8 1.3 copy.53.bias
  9.1 1.3 copy.51.upd
  10.4 1.7 copy.49.q2
  12.1 1.8 copy.50.k2
  13.9 1.9 copy.77
  15.8 12.5 %shard_map.181 = (bf16[1024,128]{1,0:T(8,128)(2,1)}, bf16[1024,64]{1,0:T(8,128)(2,1)}, f32[1024,128]{1,0:T(8,128)}, f32[1024,128]{1,0:T(8,128)}, bf16[384,128]{1,0:T(8,128)(2,1)}) custom-call(bf16[1024,128]{1,0:T(8,128)(2,1)} %q1.1, bf16[1024,128]{1,0:T(8,128)(2,1)} %k1.1, bf16[1024,64]{1,0:T(8,128)(2,1)} %copy.49.q2, bf16[1024,64]{1,0:T(8,128)(2,1)} %copy.50.k2, ...), custom_call_target="tpu_custom_call" | custom-call | flops 2000000000 | bytes 4000000 | tf_op jit(solution)/shard_map/pallas_call | solution.py:181
  28.3 12.5 %all-gather = bf16[1536,128]{1,0:T(8,128)(2,1)S(1)} all-gather(bf16[384,128]{1,0:T(8,128)(2,1)} %get-tuple-element.12), channel_id=2, replica_groups=mesh['sp_0'=4,'sp_1'=4,'tp'=8] {'sp_1'}, dimensions={0}, use_global_device_ids=true | all-gather | bytes 491520 | tf_op jit(solution)/shard_map/all_gather | solution.py:238
  40.7 0.8 fusion.53
  41.5 0.8 fusion.121
  44.8 0.1 convolution_add_fusion.23
  47.4 0.1 convolution_add_fusion.26
  47.5 0.1 convolution_add_fusion.14
  47.7 0.1 convolution_add_fusion.11
  47.8 0.7 fusion.115
  48.6 1.5 fusion.119
  57.5 0.1 convolution_add_fusion.22
  57.7 1.0 fusion.31
  58.6 0.1 convolution_add_fusion.25
  58.8 0.1 convolution_add_fusion.13
  58.9 1.0 fusion.33
  59.9 0.1 fusion.23
  60.0 0.1 convolution_add_fusion.10
  60.1 0.1 fusion.22
  60.3 1.3 fusion.103
  61.6 0.1 pad.7
  61.7 0.1 maximum_bitcast_fusion
  61.8 10.8 %all_gather.18 = bf16[4,384,128]{2,1,0:T(8,128)(2,1)S(1)} all-gather(bf16[1,384,128]{2,1,0:T(8,128)(2,1)S(1)} %pad_maximum_fusion.4), channel_id=1, replica_groups=mesh['sp_0'=4,'sp_1'=4,'tp'=8] {'sp_0'}, dimensions={0}, use_global_device_ids=true | all-gather | bytes 491520 | tf_op jit(solution)/shard_map/all_gather | solution.py:243
  72.6 0.1 fusion.57
  72.7 0.7 fusion.116
  73.4 0.7 fusion.118
  76.6 0.1 fusion.29
  76.8 0.1 fusion.18
  76.9 0.7 fusion.117
  82.6 0.1 fusion.28
  82.7 0.1 fusion.17
  82.8 0.1 fusion.16
  83.0 0.1 fusion.27
  83.1 0.9 fusion.26
  84.0 0.1 fusion.15
  84.1 0.9 fusion.25
  85.0 0.1 fusion.14
  85.2 1.4 multiply_reduce_fusion.2
  86.7 1.2 multiply_reduce_fusion.1
  87.9 0.4 fusion.44
  88.4 0.5 copy.58
  89.0 19.1 %all_to_all.20 = bf16[1024,2,128]{2,1,0:T(2,128)(2,1)S(1)} all-to-all(bf16[1024,2,128]{2,1,0:T(2,128)(2,1)S(1)} %copy.58), channel_id=1, replica_groups=mesh['sp_0'=4,'sp_1'=4,'tp'=8] {'tp'}, dimensions={0} | all-to-all | bytes 1048576 | tf_op jit(solution)/shard_map/all_to_all | solution.py:337
  108.2 0.3 copy.60
  108.5 4.8 %multiply_reduce_fusion = (f32[128]{0:T(128)S(1)}, f32[128,2048]{1,0:T(8,128)S(1)}) fusion(bf16[128,2048]{0,1:T(8,128)(2,1)S(1)} %bitcast.206, bf16[2048,2048]{1,0:T(8,128)(2,1)} %param.32, bf16[128,2048]{1,0:T(8,128)(2,1)S(1)} %copy-done.1), kind=kOutput, calls=%fused_computation.68 | convolution fusion | flops 1074790272 | bytes 10486272 | tf_op jit(solution)/shard_map/dot_general | solution.py:339
  113.4 1.0 multiply_convert_fusion.2
  114.3 0.2 all-gather.6.cloned.1.call-start
  114.6 0.9 pad_maximum_fusion.2
  115.5 30.6 %all-gather.4.cloned.1.call-done = bf16[1024,2048]{1,0:T(8,128)(2,1)} async-done(((bf16[128,2048]{1,0:T(8,128)(2,1)}), bf16[1024,2048]{1,0:T(8,128)(2,1)}) %all-gather.4.cloned.1.call-update) | async-done | bytes 4194320 | tf_op jit(solution)/shard_map/all_gather | solution.py:347
  146.1 77.3 %all-gather.6.cloned.1.call-done = bf16[2048,2304]{1,0:T(8,128)(2,1)} async-done(((bf16[128,2304]{1,0:T(8,128)(2,1)}), bf16[2048,2304]{1,0:T(8,128)(2,1)}) %all-gather.6.cloned.1.call-update) | async-done | bytes 9437200 | tf_op jit(solution)/shard_map/all_gather | solution.py:308
  223.4 6.7 %fusion.5 = bf16[1024,768]{1,0:T(8,128)(2,1)S(1)} fusion(bf16[1024,2048]{1,0:T(8,128)(2,1)} %all-gather.4.cloned.1.call-done, bf16[2048,2304]{1,0:T(8,128)(2,1)} %all-gather.6.cloned.1.call-done), kind=kOutput, calls=%fused_computation.9 | convolution fusion | flops 3222011904 | bytes 8912896 | tf_op jit(solution)/shard_map/dot_general | solution.py:348
  230.1 0.3 copy-done.15
  230.4 3.4 %fusion.8 = bf16[1024,768]{1,0:T(8,128)(2,1)S(1)} fusion(bf16[1024,2048]{1,0:T(8,128)(2,1)S(1)} %copy-done.15, bf16[2048,2304]{1,0:T(8,128)(2,1)S(1)} %copy-done.14), kind=kOutput, calls=%fused_computation.10 | convolution fusion | flops 3222011904 | bytes 8912896 | tf_op jit(solution)/shard_map/dot_general | solution.py:349
  233.9 3.1 %collective-permute-start.1 = (bf16[2,768]{1,0:T(2,128)(2,1)S(1)}, bf16[2,768]{1,0:T(2,128)(2,1)S(1)}, u32[]{:S(2)}, u32[]{:S(2)}) collective-permute-start(bf16[2,768]{1,0:T(2,128)(2,1)S(1)} %slice.476), channel_id=1, source_target_pairs={{0,8},{8,16},{16,24},{24,32},{32,40},{40,48},{48,56},{56,64},{64,7... | collective-permute-start | bytes 9224 | tf_op jit(solution)/shard_map/ppermute | solution.py:263
  237.0 3.1 %collective-permute-start = (bf16[2,768]{1,0:T(2,128)(2,1)S(1)}, bf16[2,768]{1,0:T(2,128)(2,1)S(1)}, u32[]{:S(2)}, u32[]{:S(2)}) collective-permute-start(bf16[2,768]{1,0:T(2,128)(2,1)S(1)} %slice.469), channel_id=1, source_target_pairs={{0,8},{8,16},{16,24},{24,32},{32,40},{40,48},{48,56},{56,64},{64,7... | collective-permute-start | bytes 9224 | tf_op jit(solution)/shard_map/ppermute | solution.py:263
  240.2 0.7 collective-permute-done
  240.8 5.9 %convolution_convert_fusion = bf16[1024,2048]{1,0:T(8,128)(2,1)S(1)} fusion(bf16[2048,2304]{1,0:T(8,128)(2,1)S(1)} %copy-done.14, bf16[1024,768]{1,0:T(8,128)(2,1)S(1)} %fusion.8, bf16[1024,768]{1,0:T(8,128)(2,1)S(1)} %fusion.5, bf16[2,768]{1,0:T(2,128)(2,1)S(1)} %collective-permute-done.1, bf16[2,768]{1,0:T(2,128)(2,1)S(1)} %collective-permute-done, ...), kind=kOutput, calls=%fused_computation.1 | convolution fusion | flops 3250061312 | bytes 10516480 | tf_op jit(solution)/shard_map/dot_general | solution.py:358
  246.7 54.7 %all_to_all.21 = bf16[8,128,2048]{2,1,0:T(8,128)(2,1)S(1)} all-to-all(bf16[8,128,2048]{2,1,0:T(8,128)(2,1)S(1)} %bitcast.205), channel_id=1, replica_groups=mesh['sp_0'=4,'sp_1'=4,'tp'=8] {'tp'}, dimensions={0} | all-to-all | bytes 8388608 | tf_op jit(solution)/shard_map/all_to_all | solution.py:274
  301.4 0.7 convert_reduce_fusion
  302.1 0.9 add_convert_fusion
  (45 shorter events, 0.3 us)
Async XLA Ops:
  6.5 139.6 %all-gather.4.cloned.1.call-start = ((), (), s32[]{:S(2)}) async-start(), calls=%async_computation.2 | async-start | bytes 4718592 | tf_op jit(solution)/shard_map/all_gather | solution.py:347
  28.3 19.5 %copy-start = (bf16[1024,2,128]{2,1,0:T(2,128)(2,1)S(1)}, bf16[1024,2,128]{2,1,0:T(2,128)(2,1)}, u32[]{:S(2)}) copy-start(bf16[1024,2,128]{2,1,0:T(2,128)(2,1)} %param.25) | copy-start | bytes 1572868
  41.5 6.1 %copy-start.5 = (f32[384,128]{1,0:T(8,128)}, f32[384,128]{1,0:T(8,128)S(1)}, u32[]{:S(2)}) copy-start(f32[384,128]{1,0:T(8,128)S(1)} %get-tuple-element.34) | copy-start | bytes 589828
  41.5 6.1 %copy-start.6 = (f32[384,128]{1,0:T(8,128)}, f32[384,128]{1,0:T(8,128)S(1)}, u32[]{:S(2)}) copy-start(f32[384,128]{1,0:T(8,128)S(1)} %get-tuple-element.33) | copy-start | bytes 589828
  41.5 17.1 %copy-start.4 = (f32[384,128]{1,0:T(8,128)}, f32[384,128]{1,0:T(8,128)S(1)}, u32[]{:S(2)}) copy-start(f32[384,128]{1,0:T(8,128)S(1)} %get-tuple-element.35) | copy-start | bytes 589828
  47.8 37.4 %copy-start.3 = (f32[1024,128]{1,0:T(8,128)S(1)}, f32[1024,128]{1,0:T(8,128)}, u32[]{:S(2)}) copy-start(f32[1024,128]{1,0:T(8,128)} %get-tuple-element.10) | copy-start | bytes 1572868
  58.8 27.9 %copy-start.2 = (f32[1024,128]{1,0:T(8,128)S(1)}, f32[1024,128]{1,0:T(8,128)}, u32[]{:S(2)}) copy-start(f32[1024,128]{1,0:T(8,128)} %get-tuple-element.13) | copy-start | bytes 1572868
  58.8 27.9 %copy-start.7 = (bf16[1024,64]{1,0:T(8,128)(2,1)S(1)}, bf16[1024,64]{1,0:T(8,128)(2,1)}, u32[]{:S(2)}) copy-start(bf16[1024,64]{1,0:T(8,128)(2,1)} %get-tuple-element.14) | copy-start | bytes 393220
  72.6 15.3 %copy-start.13 = (f32[128]{0:T(128)S(1)}, f32[128]{0:T(128)}, u32[]{:S(2)}) copy-start(f32[128]{0:T(128)} %param.31) | copy-start | bytes 1540
  88.4 20.1 %copy-start.1 = (bf16[128,2048]{1,0:T(8,128)(2,1)S(1)}, bf16[128,2048]{1,0:T(8,128)(2,1)}, u32[]{:S(2)}) copy-start(bf16[128,2048]{1,0:T(8,128)(2,1)} %param.19) | copy-start | bytes 1572868
  108.5 4.9 %copy-start.12 = (f32[2048]{0:T(1024)S(1)}, f32[2048]{0:T(1024)}, u32[]{:S(2)}) copy-start(f32[2048]{0:T(1024)} %param.33) | copy-start | bytes 24580
  108.5 6.1 %copy-start.8 = (bf16[128,768]{1,0:T(8,128)(2,1)S(1)}, bf16[128,768]{1,0:T(8,128)(2,1)}, u32[]{:S(2)}) copy-start(bf16[128,768]{1,0:T(8,128)(2,1)} %param.37) | copy-start | bytes 589828
  108.5 6.1 %copy-start.9 = (bf16[128,768]{1,0:T(8,128)(2,1)S(1)}, bf16[128,768]{1,0:T(8,128)(2,1)}, u32[]{:S(2)}) copy-start(bf16[128,768]{1,0:T(8,128)(2,1)} %param.35) | copy-start | bytes 589828
  108.5 6.1 %copy-start.10 = (bf16[128,768]{1,0:T(8,128)(2,1)S(1)}, bf16[128,768]{1,0:T(8,128)(2,1)}, u32[]{:S(2)}) copy-start(bf16[128,768]{1,0:T(8,128)(2,1)} %param.34) | copy-start | bytes 589828
  113.3 2.2 copy-start.11
  114.3 109.0 %all-gather.6.cloned.1.call-start = ((), (), s32[]{:S(2)}) async-start(), calls=%async_computation.3 | async-start | bytes 10027008 | tf_op jit(solution)/shard_map/all_gather | solution.py:308
  223.4 6.7 %copy-start.14 = (bf16[2048,2304]{1,0:T(8,128)(2,1)S(1)}, bf16[2048,2304]{1,0:T(8,128)(2,1)}, u32[]{:S(2)}) copy-start(bf16[2048,2304]{1,0:T(8,128)(2,1)} %all-gather.6.cloned.1.call-done) | copy-start | bytes 28311556
  223.4 7.0 %copy-start.15 = (bf16[1024,2048]{1,0:T(8,128)(2,1)S(1)}, bf16[1024,2048]{1,0:T(8,128)(2,1)}, u32[]{:S(2)}) copy-start(bf16[1024,2048]{1,0:T(8,128)(2,1)} %all-gather.4.cloned.1.call-done) | copy-start | bytes 12582916
  233.9 6.3 %collective-permute-start.1 = (bf16[2,768]{1,0:T(2,128)(2,1)S(1)}, bf16[2,768]{1,0:T(2,128)(2,1)S(1)}, u32[]{:S(2)}, u32[]{:S(2)}) collective-permute-start(bf16[2,768]{1,0:T(2,128)(2,1)S(1)} %slice.476), channel_id=1, source_target_pairs={{0,8},{8,16},{16,24},{24,32},{32,40},{40,48},{48,56},{56,64},{64,7... | collective-permute-start | bytes 9224 | tf_op jit(solution)/shard_map/ppermute | solution.py:263
  237.0 3.8 %collective-permute-start = (bf16[2,768]{1,0:T(2,128)(2,1)S(1)}, bf16[2,768]{1,0:T(2,128)(2,1)S(1)}, u32[]{:S(2)}, u32[]{:S(2)}) collective-permute-start(bf16[2,768]{1,0:T(2,128)(2,1)S(1)} %slice.469), channel_id=1, source_target_pairs={{0,8},{8,16},{16,24},{24,32},{32,40},{40,48},{48,56},{56,64},{64,7... | collective-permute-start | bytes 9224 | tf_op jit(solution)/shard_map/ppermute | solution.py:263
Sparse Core Ops, SparseCore 0:
  114.5 31.5 all-gather.3
  148.2 75.0 all-gather.5
where the time goes:
time: 312 us; the launch traced here: 310 us
  waiting for transfers between devices  109 us (35%)
  blocking collectives  97.1 us (31%)
  between operations  33.7 us (11%)
  matrix products  29.6 us (9%)
  local copies, waits for them, and re-layouts  15.7 us (5%)
  Pallas kernels  12.5 us (4%)
  starting transfers between devices  6.44 us (2%)
  other arithmetic  6.19 us (2%)
    all_gather x1, waiting for transfers between devices, per_device(): lax.all_gather(jnp.concatenate([switching_channel_map, broadening_channel...  77.3 us
    all_to_all x1, blocking collectives, summed_on_arrival(): lax.all_to_all(tiles, axis, split_axis=0, concat_axis=0, tiled=True)  54.7 us
    all_gather x1, waiting for transfers between devices, per_device(): features = lax.all_gather(normed, 'tp', axis=0, tiled=True)  30.6 us
    all_to_all x1, blocking collectives, per_device(): lax.all_to_all(linear_attend, 'tp', split_axis=0, concat_axis=2, tiled=True)  19.1 us
    pallas_call x1, Pallas kernels, local_recurrence(): pl.pallas_call(local_kernel, out_shape=(jax.ShapeDtypeStruct((1024, 128),...  12.5 us
    all_gather x1, blocking collectives, incoming_states(): row = lax.all_gather(pay, 'sp_1')  12.5 us
    all_gather x1, blocking collectives, incoming_states(): rows = lax.all_gather(join_pay(*whole), 'sp_0')  10.8 us
    unnamed x38, local copies, waits for them, and re-layouts  9.64 us
  transfers between devices with their start and end apart: 4, of which 3 were waited for; matrix products, arithmetic and copies ran while one was open for 0% of the time, Pallas kernels for 0%

commit v1 on v0

--- a/solution.py
+++ b/solution.py
@@ -257,31 +257,230 @@
     return (scaled * jax.nn.silu(gate_cols.astype(F32))).astype(BF16)
 
 
-def from_behind(value, axis, steps):
-    count = lax.axis_size(axis)
-    leading, last = (max(0, -steps), min(count, count - steps))
-    return lax.ppermute(value, axis, [(source, source + steps) for source in range(leading, last)])
-
-
-def split_up(shard, dim, size):
-    lengths = shard.shape
-    tiles = shard.reshape(*lengths[:dim], size, lengths[dim] // size, *lengths[dim + 1 :])
-    return jnp.moveaxis(tiles, dim, 0)
-
-
-def summed_on_arrival(shard, axis, dim):
-    tiles = split_up(shard, dim, lax.axis_size(axis))
-    arrived = lax.all_to_all(tiles, axis, split_axis=0, concat_axis=0, tiled=True)
-    return arrived.astype(jnp.float32).sum(axis=0)
-
-
-def causal_taps(edge_rows, low_rows, taps_col):
-    padded = jnp.concatenate([edge_rows, low_rows], axis=0)
-    length = low_rows.shape[0]
-    total = taps_col[0] * padded[0:length]
-    for tap_index in range(1, TAPS):
-        total = total + taps_col[tap_index] * padded[tap_index : tap_index + length]
-    return total
+MESH = pl.DeviceIdType.MESH
+WIDTH = 2048
+UNITS = 768
+
+
+def ring_places():
+    me = lax.axis_index("tp")
+    x, core = me // 2, me % 2
+    right = ((x + 1) % 4) * 2 + core
+    left = ((x + 3) % 4) * 2 + core
+    far = ((x + 2) % 4) * 2 + core
+    return me, x, core, x * 2 + 1 - core, right, left, far
+
+
+def mixer_kernel(
+    normed, skip, taps, weights,
+    out,
+    feat, wgu, wdn, low, hid, acc, d2d_out, d2d_in, far_out, msg_r, msg_l, far_in, in_l, in_r,
+    load_sem, send_sem, recv_sem,
+):
+    me, x, core, mate, right, left, far = ring_places()
+    z, y = lax.axis_index("sp_0"), lax.axis_index("sp_1")
+    place = z * 4 + y
+    after_z, after_y = ((place + 1) % 16) // 4, (place + 1) % 4
+    prior_z, prior_y = ((place + 15) % 16) // 4, (place + 15) % 4
+    to_mate, to_right, to_left = {"tp": mate}, {"tp": right}, {"tp": left}
+    to_next = {"sp_0": after_z, "sp_1": after_y}
+    to_prior = {"sp_0": prior_z, "sp_1": prior_y}
+
+    load_gu = pltpu.make_async_copy(weights.at[:, 0 : 2 * UNITS], wgu, load_sem.at[0])
+    load_dn = pltpu.make_async_copy(weights.at[:, 2 * UNITS :], wdn, load_sem.at[1])
+    load_gu.start()
+    load_dn.start()
+
+    barrier = pltpu.get_barrier_semaphore()
+    for peer in (to_mate, to_right, to_left, to_next, to_prior):
+        pl.semaphore_signal(barrier, inc=1, device_id=peer, device_id_type=MESH)
+    pl.semaphore_wait(barrier, 5)
+
+    def send(k, src, dst, peer):
+        return pltpu.make_async_remote_copy(
+            src_ref=src, dst_ref=dst, send_sem=send_sem.at[k], recv_sem=recv_sem.at[k],
+            device_id=peer, device_id_type=MESH,
+        )
+
+    def shard(i, first=0, count=128):
+        return feat.at[pl.ds(pl.multiple_of(i * 128 + first, 64), count), :]
+
+    half_a, half_b = normed.at[0:64, :], normed.at[64:128, :]
+    own_mate = send(0, normed, shard(me), to_mate)
+    own = [
+        send(1, half_a, shard(me, 0, 64), to_right),
+        send(3, half_b, shard(me, 64, 64), to_left),
+        send(2, half_b, shard(me, 64, 64), to_right),
+        send(4, half_a, shard(me, 0, 64), to_left),
+    ]
+    own_mate.start()
+    for c in own:
+        c.start()
+    a_right, b_left, b_right, a_left = own
+    fwd_a = send(5, shard(left, 0, 64), shard(left, 0, 64), to_right)
+    fwd_b = send(6, shard(right, 64, 64), shard(right, 64, 64), to_left)
+    mate_l = send(7, shard(left), shard(left), to_mate)
+    mate_r = send(8, shard(right), shard(right), to_mate)
+    mate_fa = send(9, shard(far, 0, 64), shard(far, 0, 64), to_mate)
+    mate_fb = send(10, shard(far, 64, 64), shard(far, 64, 64), to_mate)
+    halo_rows = low.at[pl.ds(1024, 16), :]
+    halo = send(11, halo_rows, low.at[pl.ds(0, 16), :], to_next)
+
+    feat[pl.ds(pl.multiple_of(me * 128, 128), 128), :] = normed[...]
+
+    def gate_up(pair):
+        rows = pl.ds(pl.multiple_of(pair * 256, 256), 256)
+        put = pl.ds(pl.multiple_of(pair * 256 + 16, 16), 256)
+
+        def tile(j, carry):
+            cols = pl.ds(pl.multiple_of(j * 256, 256), 256)
+            low[put, cols] = mm(feat[rows, :], wgu[:, cols]).astype(BF16)
+            return carry
+
+        lax.fori_loop(0, 6, tile, 0)
+
+        @pl.when(pair == 3)
+        def _():
+            halo.start()
+
+    load_gu.wait()
+    own_mate.wait_recv()
+    gate_up(x)
+    a_right.wait_recv()
+    fwd_a.start()
+    b_left.wait_recv()
+    fwd_b.start()
+    b_right.wait_recv()
+    mate_l.start()
+    a_left.wait_recv()
+    mate_r.start()
+    mate_r.wait_recv()
+    gate_up((x + 1) % 4)
+    mate_l.wait_recv()
+    gate_up((x + 3) % 4)
+    fwd_a.wait_recv()
+    mate_fa.start()
+    fwd_b.wait_recv()
+    mate_fb.start()
+    mate_fa.wait_recv()
+    mate_fb.wait_recv()
+    gate_up((x + 2) % 4)
+    load_dn.wait()
+    halo.wait_recv()
+
+    @pl.when(place == 0)
+    def _():
+        low[0:16, :] = jnp.zeros((16, 2 * UNITS), BF16)
+
+    def conv(cols, pair, side):
+        rows = pl.ds(pl.multiple_of(pair * 256, 256), 272)
+        lows = low[rows, pl.ds(pl.multiple_of(cols + side * UNITS, 128), 128)].astype(F32)
+        span = pl.ds(pl.multiple_of(cols, 128), 128)
+        t = [taps[j, side : side + 1, span].astype(F32) for j in range(3)]
+        total = t[0] * pltpu.roll(lows, 2, 0) + t[1] * pltpu.roll(lows, 1, 0) + t[2] * lows
+        return total[16:]
+
+    def down(k, pair):
+        def mix(j, carry):
+            g = conv(j * 128, pair, 0)
+            u = conv(j * 128, pair, 1)
+            span = pl.ds(pl.multiple_of(j * 128, 128), 128)
+            hid[:, span] = (g / (1.0 + jnp.exp(-g)) * u).astype(BF16)
+            return carry
+
+        lax.fori_loop(0, 6, mix, 0)
+        mine = pl.ds(pl.multiple_of(core * 128, 128), 128)
+        other = pl.ds(pl.multiple_of((1 - core) * 128, 128), 128)
+
+        def tile(j, carry):
+            span = pl.ds(pl.multiple_of(j * 256, 256), 256)
+            both = jnp.concatenate([hid[mine, :], hid[other, :]], axis=0)
+            made = mm_nt(both, wdn[span, :])
+            acc[k, :, span] = made[:128]
+            d2d_out[k, :, span] = made[128:].astype(BF16)
+            return carry
+
+        lax.fori_loop(0, 8, tile, 0)
+        pair_sum = send(12 + k, d2d_out.at[k], d2d_in.at[k], to_mate)
+        pair_sum.start()
+        return pair_sum
+
+    far_a = send(16, far_out.at[0:64, :], far_in.at[0:64, :], to_right)
+    far_b = send(17, far_out.at[64:128, :], far_in.at[64:128, :], to_left)
+    r_b = send(18, msg_r.at[64:128, :], in_l.at[64:128, :], to_right)
+    r_a = send(19, msg_r.at[0:64, :], in_l.at[0:64, :], to_right)
+    l_a = send(20, msg_l.at[0:64, :], in_r.at[0:64, :], to_left)
+    l_b = send(21, msg_l.at[64:128, :], in_r.at[64:128, :], to_left)
+
+    d_far = down(0, (x + 2) % 4)
+    d_right = down(1, (x + 1) % 4)
+    d_far.wait_recv()
+    far_out[...] = (acc[0] + d2d_in[0].astype(F32)).astype(BF16)
+    far_a.start()
+    far_b.start()
+    d_left = down(2, (x + 3) % 4)
+    d_right.wait_recv()
+    msg_r[64:128, :] = (acc[1, 64:128, :] + d2d_in[1, 64:128, :].astype(F32)).astype(BF16)
+    r_b.start()
+    d_left.wait_recv()
+    msg_l[0:64, :] = (acc[2, 0:64, :] + d2d_in[2, 0:64, :].astype(F32)).astype(BF16)
+    l_a.start()
+    d_own = down(3, x)
+    far_a.wait_recv()
+    msg_r[0:64, :] = (
+        acc[1, 0:64, :] + d2d_in[1, 0:64, :].astype(F32) + far_in[0:64, :].astype(F32)
+    ).astype(BF16)
+    r_a.start()
+    far_b.wait_recv()
+    msg_l[64:128, :] = (
+        acc[2, 64:128, :] + d2d_in[2, 64:128, :].astype(F32) + far_in[64:128, :].astype(F32)
+    ).astype(BF16)
+    l_b.start()
+    d_own.wait_recv()
+    acc[3] = acc[3] + d2d_in[3].astype(F32) + skip[...]
+    for c in (r_b, l_a, r_a, l_b):
+        c.wait_recv()
+    out[...] = (acc[3] + in_l[...].astype(F32) + in_r[...].astype(F32)).astype(BF16)
+
+    for c in (own_mate, *own, fwd_a, fwd_b, mate_l, mate_r, mate_fa, mate_fb, halo):
+        c.wait_send()
+    for c in (d_far, d_right, d_left, d_own, far_a, far_b, r_b, r_a, l_a, l_b):
+        c.wait_send()
+
+
+def channel_mixer(normed, skip, taps, weights):
+    vm = pl.BlockSpec(memory_space=pltpu.VMEM)
+    return pl.pallas_call(
+        mixer_kernel,
+        out_shape=jax.ShapeDtypeStruct((128, WIDTH), BF16),
+        in_specs=[vm, vm, vm, pl.BlockSpec(memory_space=pl.ANY)],
+        out_specs=vm,
+        scratch_shapes=[
+            pltpu.VMEM((1024, WIDTH), BF16),
+            pltpu.VMEM((WIDTH, 2 * UNITS), BF16),
+            pltpu.VMEM((WIDTH, UNITS), BF16),
+            pltpu.VMEM((1040, 2 * UNITS), BF16),
+            pltpu.VMEM((256, UNITS), BF16),
+            pltpu.VMEM((4, 128, WIDTH), F32),
+            pltpu.VMEM((4, 128, WIDTH), BF16),
+            pltpu.VMEM((4, 128, WIDTH), BF16),
+            pltpu.VMEM((128, WIDTH), BF16),
+            pltpu.VMEM((128, WIDTH), BF16),
+            pltpu.VMEM((128, WIDTH), BF16),
+            pltpu.VMEM((128, WIDTH), BF16),
+            pltpu.VMEM((128, WIDTH), BF16),
+            pltpu.VMEM((128, WIDTH), BF16),
+            pltpu.SemaphoreType.DMA((2,)),
+            pltpu.SemaphoreType.DMA((22,)),
+            pltpu.SemaphoreType.DMA((22,)),
+        ],
+        compiler_params=pltpu.CompilerParams(
+            collective_id=1, has_side_effects=True, vmem_limit_bytes=60 * 1024 * 1024
+        ),
+        cost_estimate=pl.CostEstimate(
+            flops=10_000_000_000, bytes_accessed=12_000_000, transcendentals=1_000_000
+        ),
+    )(normed, skip, taps, weights)
 
 
 def per_device(
@@ -344,24 +543,7 @@
         * lax.rsqrt(jnp.mean(skip_stream * skip_stream, axis=-1, keepdims=True) + EPSILON)
         * channel_normalizer_coef
     ).astype(jnp.bfloat16)
-    features = lax.all_gather(normed, "tp", axis=0, tiled=True)
-    gate_full = jnp.dot(features, gathered[:, :768], preferred_element_type=jnp.float32)
-    up_full = jnp.dot(features, gathered[:, 768:1536], preferred_element_type=jnp.float32)
-    gate_low = gate_full.astype(jnp.bfloat16)
-    up_low = up_full.astype(jnp.bfloat16)
-    edge_gate, edge_up = from_behind((gate_low[-(TAPS - 1) :], up_low[-(TAPS - 1) :]), SP, 1)
-    taps = timewise_convolve_tapvalues.astype(jnp.float32)
-    gate_conv = causal_taps(edge_gate, gate_low, taps[:, 0])
-    up_conv = causal_taps(edge_up, up_low, taps[:, 1])
-    hidden = (jax.nn.silu(gate_conv) * up_conv).astype(jnp.bfloat16)
-    down_sum = summed_on_arrival(
-        lax.dot_general(
-            hidden, gathered[:, 1536:], (((1,), (1,)), ((), ())), preferred_element_type=jnp.float32
-        ).astype(jnp.bfloat16),
-        "tp",
-        0,
-    )
-    return (skip_stream + down_sum).astype(jnp.bfloat16)
+    return channel_mixer(normed, skip_stream, timewise_convolve_tapvalues, gathered)
 
 
 def solution(mesh):

time: 312 us -> 187 us (0.60)
  waiting for transfers between devices: 109 us -> 0.02 us
  Pallas kernels: 12.5 us -> 73.8 us
  blocking collectives: 97.1 us -> 44.3 us
  matrix products: 29.6 us -> 13.3 us
  starting transfers between devices: 6.44 us -> 0.01 us
    all_gather x1, waiting for transfers between devices: 77.3 us -> 0.01 us  [per_device(): lax.all_gather(jnp.concatenate([switching_channel_map, broadening_channel...]
    pallas_call x0 -> x1, Pallas kernels: none -> 61.2 us  [channel_mixer(): pl.pallas_call(mixer_kernel, out_shape=jax.ShapeDtypeStruct((128, WIDTH),...]
    all_to_all x1 -> x0, blocking collectives: 54.7 us -> none  [summed_on_arrival(): lax.all_to_all(tiles, axis, split_axis=0, concat_axis=0, tiled=True)]
    all_gather x1 -> x0, waiting for transfers between devices: 30.6 us -> none  [per_device(): features = lax.all_gather(normed, 'tp', axis=0, tiled=True)]
    dot_general x3 -> x0, matrix products: 16 us -> none  [the longest x1 6.7 us: per_device(): jnp.dot(features, gathered[:, :768], preferred_element_type=jnp.float32)]
    ppermute x2 -> x0, starting transfers between devices: 6.22 us -> none  [from_behind(): lax.ppermute(value, axis, [(source, source + steps) for source in range(l...]
    all_gather x1, blocking collectives: 10.8 us -> 14.1 us  [incoming_states(): rows = lax.all_gather(join_pay(*whole), 'sp_0')]
    unnamed x38 -> x25, local copies, waits for them, and re-layouts: 9.64 us -> 11.2 us
  transfers between devices with their start and end apart: 4 -> 1, of which waited for: 3 -> 0; matrix products, arithmetic and copies ran while one was open for 0% -> 17% of each run, Pallas kernels for 0% -> 7%
where the time goes in v1:
time: 187 us; the launch traced here: 186 us
  Pallas kernels  73.8 us (39%)
  blocking collectives  44.3 us (24%)
  between operations  33.1 us (18%)
  local copies, waits for them, and re-layouts  16.2 us (9%)
  matrix products  13.3 us (7%)
  other arithmetic  5.16 us (3%)
    pallas_call x1, Pallas kernels, channel_mixer(): pl.pallas_call(mixer_kernel, out_shape=jax.ShapeDtypeStruct((128, WIDTH),...  61.2 us
    all_to_all x1, blocking collectives, per_device(): lax.all_to_all(linear_attend, 'tp', split_axis=0, concat_axis=2, tiled=True)  17.4 us
    all_gather x1, blocking collectives, incoming_states(): rows = lax.all_gather(join_pay(*whole), 'sp_0')  14.1 us
    all_gather x1, blocking collectives, incoming_states(): row = lax.all_gather(pay, 'sp_1')  12.8 us
    pallas_call x1, Pallas kernels, local_recurrence(): pl.pallas_call(local_kernel, out_shape=(jax.ShapeDtypeStruct((1024, 128),...  12.6 us
    unnamed x25, local copies, waits for them, and re-layouts  11.2 us
    dot_general x24, matrix products, mm(): return jnp.dot(a.astype(BF16), b.astype(BF16), preferred_element_type=F32)  8.54 us
    dot_general x1, matrix products, per_device(): jnp.dot(arrived.reshape(row_count, -1), emission_map_weights, preferred_e...  4.74 us
  transfers between devices with their start and end apart: 1, of which 0 were waited for; matrix products, arithmetic and copies ran while one was open for 17% of the time, Pallas kernels for 7%

profile of v1, /device:TPU:1, one launch (start us, length us, event | category | flops | bytes accessed | tf_op | source)
XLA Modules:
  0.0 185.8 jit_solution(5548134113973621677)
XLA Ops:
  6.5 0.0 all-gather.3.cloned.1.call-start
  6.5 2.0 %pad_maximum_fusion = bf16[128,2304]{1,0:T(8,128)(2,1)} fusion(bf16[128,768]{1,0:T(8,128)(2,1)} %param.37, bf16[128,768]{1,0:T(8,128)(2,1)} %param.35, bf16[128,768]{1,0:T(8,128)(2,1)} %param.34), kind=kLoop, calls=%fused_computation.54 | loop fusion | flops 1769472 | bytes 1179648 | tf_op jit(solution)/shard_map/concatenate | solution.py:508
  8.5 0.0 all-gather.3.cloned.1.call-update
  8.5 1.9 %copy.77 = bf16[128,8,2,128]{3,1,2,0:T(8,128)(2,1)} copy(bf16[128,8,2,128]{3,2,1,0:T(2,128)(2,1)} %bitcast.204) | data formatting | bytes 1048576
  10.5 1.7 copy.49.q2
  12.2 1.7 copy.50.k2
  13.9 1.3 copy.51.upd
  15.2 1.3 copy.52.level
  16.5 1.2 copy.53.bias
  17.8 12.6 %shard_map.181 = (bf16[1024,128]{1,0:T(8,128)(2,1)}, bf16[1024,64]{1,0:T(8,128)(2,1)}, f32[1024,128]{1,0:T(8,128)}, f32[1024,128]{1,0:T(8,128)}, bf16[384,128]{1,0:T(8,128)(2,1)}) custom-call(bf16[1024,128]{1,0:T(8,128)(2,1)} %q1.1, bf16[1024,128]{1,0:T(8,128)(2,1)} %k1.1, bf16[1024,64]{1,0:T(8,128)(2,1)} %copy.49.q2, bf16[1024,64]{1,0:T(8,128)(2,1)} %copy.50.k2, ...), custom_call_target="tpu_custom_call" | custom-call | flops 2000000000 | bytes 4000000 | tf_op jit(solution)/shard_map/pallas_call | solution.py:181
  30.3 12.8 %all-gather = bf16[1536,128]{1,0:T(8,128)(2,1)S(1)} all-gather(bf16[384,128]{1,0:T(8,128)(2,1)} %get-tuple-element.12), channel_id=2, replica_groups=mesh['sp_0'=4,'sp_1'=4,'tp'=8] {'sp_1'}, dimensions={0}, use_global_device_ids=true | all-gather | bytes 491520 | tf_op jit(solution)/shard_map/all_gather | solution.py:238
  43.1 0.1 fusion.40
  43.2 0.7 fusion.106
  46.4 0.7 fusion.104
  56.9 1.3 fusion.90
  58.3 0.1 convolution_add_fusion.23
  58.4 0.1 convolution_add_fusion.22
  58.5 0.1 fusion.18
  58.7 0.1 pad.7
  58.7 0.1 maximum_bitcast_fusion
  58.8 0.1 convolution_add_fusion.26
  59.0 0.1 convolution_add_fusion.25
  59.1 0.1 fusion.20
  59.2 0.1 convolution_add_fusion.11
  59.4 0.1 convolution_add_fusion.10
  59.5 0.1 fusion.9
  59.6 0.1 convolution_add_fusion.14
  59.8 0.1 convolution_add_fusion.13
  59.9 0.1 fusion.10
  60.1 0.0 copy-start.2
  60.1 14.1 %all_gather.15 = bf16[4,384,128]{2,1,0:T(8,128)(2,1)S(1)} all-gather(bf16[1,384,128]{2,1,0:T(8,128)(2,1)S(1)} %pad_maximum_fusion.2), channel_id=1, replica_groups=mesh['sp_0'=4,'sp_1'=4,'tp'=8] {'sp_0'}, dimensions={0}, use_global_device_ids=true | all-gather | bytes 491520 | tf_op jit(solution)/shard_map/all_gather | solution.py:243
  74.2 0.1 fusion.44
  74.3 0.0 copy-start.6
  74.3 0.7 fusion.103
  77.5 0.6 fusion.101
  79.2 0.6 fusion.102
  83.3 0.1 fusion.16
  83.4 0.1 fusion.15
  83.6 0.1 fusion.14
  83.7 0.1 fusion.13
  83.8 0.1 fusion.12
  84.0 0.0 copy-done.4
  84.0 0.0 copy-done.5
  84.0 1.6 multiply_reduce_fusion.1
  85.6 1.0 fusion.5
  86.6 1.0 fusion.4
  87.6 1.0 fusion.3
  88.5 0.1 fusion.2
  88.7 0.1 fusion.1
  88.8 0.0 copy-done.3
  88.8 1.5 multiply_reduce_fusion.2
  90.3 0.7 fusion.100
  91.1 0.4 fusion.31
  91.5 0.1 pad_maximum_fusion.1
  91.5 0.5 copy.58
  92.1 17.4 %all_to_all.15 = bf16[1024,2,128]{2,1,0:T(2,128)(2,1)S(1)} all-to-all(bf16[1024,2,128]{2,1,0:T(2,128)(2,1)S(1)} %copy.58), channel_id=1, replica_groups=mesh['sp_0'=4,'sp_1'=4,'tp'=8] {'tp'}, dimensions={0} | all-to-all | bytes 1048576 | tf_op jit(solution)/shard_map/all_to_all | solution.py:536
  109.5 0.1 copy.59
  109.6 0.3 copy.60
  109.9 0.0 copy-start.7
  109.9 4.7 %multiply_reduce_fusion = (f32[128]{0:T(128)S(1)}, f32[128,2048]{1,0:T(8,128)S(1)}) fusion(bf16[128,2048]{0,1:T(8,128)(2,1)S(1)} %bitcast.202, bf16[2048,2048]{1,0:T(8,128)(2,1)} %param.32, bf16[128,2048]{1,0:T(8,128)(2,1)S(1)} %copy-done.2), kind=kOutput, calls=%fused_computation.49 | convolution fusion | flops 1074790272 | bytes 10486272 | tf_op jit(solution)/shard_map/dot_general | solution.py:538
  114.7 1.1 multiply_convert_fusion.normed
  115.8 0.0 copy-done
  115.8 61.2 %shard_map.182 = bf16[128,2048]{1,0:T(8,128)(2,1)} custom-call(bf16[128,2048]{1,0:T(8,128)(2,1)} %multiply_convert_fusion.normed, f32[128,2048]{1,0:T(8,128)} %copy-done, bf16[3,2,768]{2,1,0:T(2,128)(2,1)} %taps.1, bf16[2048,2304]{1,0:T(8,128)(2,1)} %all-gather.3.cloned.1.call-done.weights), custom_call_target="tpu_custom_call" | custom-call | flops 10000000000 | bytes 12000000 | tf_op jit(solution)/shard_map/pallas_call | solution.py:453
  177.0 1.9 %copy.79 = bf16[128,2048]{1,0:T(8,128)(2,1)} copy(bf16[128,2048]{1,0:T(8,128)(2,1)} %shard_map.182) | data formatting | bytes 1048576
  (16 shorter events, 0.0 us)
Async XLA Ops:
  6.5 109.2 %all-gather.3.cloned.1.call-start = ((), (), s32[]{:S(2)}) async-start(), calls=%async_computation.1 | async-start | bytes 10027008 | tf_op jit(solution)/shard_map/all_gather | solution.py:507
  17.8 72.6 %copy-start.1 = (bf16[1024,2,128]{2,1,0:T(2,128)(2,1)S(1)}, bf16[1024,2,128]{2,1,0:T(2,128)(2,1)}, u32[]{:S(2)}) copy-start(bf16[1024,2,128]{2,1,0:T(2,128)(2,1)} %param.25) | copy-start | bytes 1572868
  30.3 58.5 %copy-start.3 = (f32[1024,128]{1,0:T(8,128)S(1)}, f32[1024,128]{1,0:T(8,128)}, u32[]{:S(2)}) copy-start(f32[1024,128]{1,0:T(8,128)} %get-tuple-element.10) | copy-start | bytes 1572868
  30.3 60.7 %copy-start.8 = (f32[128]{0:T(128)S(1)}, f32[128]{0:T(128)}, u32[]{:S(2)}) copy-start(f32[128]{0:T(128)} %param.31) | copy-start | bytes 1540
  60.1 49.8 %copy-start.2 = (bf16[128,2048]{1,0:T(8,128)(2,1)S(1)}, bf16[128,2048]{1,0:T(8,128)(2,1)}, u32[]{:S(2)}) copy-start(bf16[128,2048]{1,0:T(8,128)(2,1)} %param.19) | copy-start | bytes 1572868
  74.3 9.6 %copy-start.4 = (f32[1,384,128]{2,1,0:T(8,128)}, f32[1,384,128]{2,1,0:T(8,128)S(1)}, u32[]{:S(2)}) copy-start(f32[1,384,128]{2,1,0:T(8,128)S(1)} %get-tuple-element.22) | copy-start | bytes 589828
  74.3 9.6 %copy-start.5 = (f32[1,384,128]{2,1,0:T(8,128)}, f32[1,384,128]{2,1,0:T(8,128)S(1)}, u32[]{:S(2)}) copy-start(f32[1,384,128]{2,1,0:T(8,128)S(1)} %get-tuple-element.21) | copy-start | bytes 589828
  74.3 9.6 %copy-start.6 = (f32[1,384,128]{2,1,0:T(8,128)}, f32[1,384,128]{2,1,0:T(8,128)S(1)}, u32[]{:S(2)}) copy-start(f32[1,384,128]{2,1,0:T(8,128)S(1)} %get-tuple-element.20) | copy-start | bytes 589828
  109.9 4.8 %copy-start.7 = (f32[2048]{0:T(1024)S(1)}, f32[2048]{0:T(1024)}, u32[]{:S(2)}) copy-start(f32[2048]{0:T(1024)} %param.33) | copy-start | bytes 24580
  114.7 1.2 copy-start
Sparse Core Ops, SparseCore 0:
  9.5 81.8 all-gather.2

commit v2 on v1

--- a/solution.py
+++ b/solution.py
@@ -6,9 +6,11 @@
 from jax.sharding import Mesh
 from jax.sharding import PartitionSpec as P
 
-TAPS = 3
 SP = ("sp_0", "sp_1")
 SP_TP = ("sp_0", "sp_1", "tp")
+MESH = pl.DeviceIdType.MESH
+WIDTH = 2048
+UNITS = 768
 
 BLK = 128
 NBLK = 8
@@ -94,13 +96,133 @@
     return extra
 
 
-def local_kernel(
-    q1, k1, q2, k2, vals, upd, fade, boost, level, bias,
-    r1, r2, o1, o2, pay,
-    beta_s, cum_s, keep_s, qd1, qd2, loc1, loc2, add1, add2,
+def ring_places():
+    me = lax.axis_index("tp")
+    x, core = me // 2, me % 2
+    right = ((x + 1) % 4) * 2 + core
+    left = ((x + 3) % 4) * 2 + core
+    far = ((x + 2) % 4) * 2 + core
+    return me, x, core, x * 2 + 1 - core, right, left, far
+
+
+def read_maps(pays, i):
+    low = pays[i, 320:384, :].astype(F32)
+    g1 = low[0:1, 64:65] + low[1:2, 64:65]
+    g2 = low[2:3, 64:65] + low[3:4, 64:65]
+    one = (pays[i, 0:128, :], pays[i, 128:256, :].astype(F32), g1)
+    two = (pays[i, 320:384, :][:, :64], pays[i, 256:320, :].astype(F32), g2)
+    return one, two
+
+
+def after(earlier, later):
+    d0, a0, g0 = earlier
+    d1, a1, g1 = later
+    made = mm(d1, jnp.concatenate([a0, d0], axis=1))
+    return (
+        d0 * g1 + d1.astype(F32) * g0 + made[:, BLK:],
+        a0 * g1 + a1 + made[:, :BLK],
+        g0 * g1,
+    )
+
+
+def write_maps(pays, i, one, two):
+    (d1, a1, g1), (d2, a2, g2) = one, two
+    row = lax.broadcasted_iota(jnp.int32, (64, 64), 0)
+    hi1, hi2 = g1.astype(BF16).astype(F32), g2.astype(BF16).astype(F32)
+    scal = jnp.where(row == 0, jnp.broadcast_to(hi1, (64, 64)), 0.0)
+    scal = scal + jnp.where(row == 1, jnp.broadcast_to(g1 - hi1, (64, 64)), 0.0)
+    scal = scal + jnp.where(row == 2, jnp.broadcast_to(hi2, (64, 64)), 0.0)
+    scal = scal + jnp.where(row == 3, jnp.broadcast_to(g2 - hi2, (64, 64)), 0.0)
+    pays[i, 0:128, :] = d1.astype(BF16)
+    pays[i, 128:256, :] = a1.astype(BF16)
+    pays[i, 256:320, :] = a2.astype(BF16)
+    pays[i, 320:384, :] = jnp.concatenate([d2, scal], axis=1).astype(BF16)
+
+
+def layer_kernel(
+    q1, k1, q2, k2, vals, gates, upd, fade, boost, level, bias, norm_coef,
+    emission, chan_coef, hidden, w_gate, w_up, w_down, taps,
+    out,
+    beta_s, cum_s, keep_s, qd1, qd2, loc1, loc2, add1, add2, vf, gf, r1, r2, o1, o2,
+    pays, row_pays, heads, arrived, emit_w, skip, normed, wall,
+    feat, low, hid, acc, d2d_out, d2d_in, far_out, msg_r, msg_l, far_in, in_l, in_r,
+    load_sem, send_sem, recv_sem, wsend, wrecv,
 ):
+    me, x, core, mate, right, left, far = ring_places()
+    z, y = lax.axis_index("sp_0"), lax.axis_index("sp_1")
+    place = z * 4 + y
+    after_z, after_y = ((place + 1) % 16) // 4, (place + 1) % 4
+    prior_z, prior_y = ((place + 15) % 16) // 4, (place + 15) % 4
+    to_mate, to_right, to_left = {"tp": mate}, {"tp": right}, {"tp": left}
+    to_next = {"sp_0": after_z, "sp_1": after_y}
+    to_prior = {"sp_0": prior_z, "sp_1": prior_y}
+
+    home = pl.ds(pl.multiple_of(place * 128, 128), 128)
+    loads = [
+        pltpu.make_async_copy(w_gate, wall.at[home, 0:UNITS], load_sem.at[0]),
+        pltpu.make_async_copy(w_up, wall.at[home, UNITS : 2 * UNITS], load_sem.at[1]),
+        pltpu.make_async_copy(w_down, wall.at[home, 2 * UNITS :], load_sem.at[2]),
+        pltpu.make_async_copy(emission, emit_w, load_sem.at[3]),
+    ]
+    for c in loads:
+        c.start()
+
+    step = 1 - 2 * core
+    at = (y, z)
+    names = ("sp_1", "sp_0")
+    ahead = ((y + step + 4) % 4, (z + step + 4) % 4)
+    behind = ((y - step + 4) % 4, (z - step + 4) % 4)
+    across = ((y + 2) % 4, (z + 2) % 4)
+
+    barrier = pltpu.get_barrier_semaphore()
+    peers = [{"tp": (me + i) % 8} for i in range(1, 8)]
+    peers += [{names[d]: n[d]} for d in range(2) for n in (ahead, behind)]
+    peers += [to_next, to_prior]
+    for peer in peers:
+        pl.semaphore_signal(barrier, inc=1, device_id=peer, device_id_type=MESH)
+
+    def ring_copy(sems, k, kind, ref_at, dim):
+        src = ref_at(behind[dim] if kind == 2 else at[dim])
+        goal = behind[dim] if kind == 1 else ahead[dim]
+        return pltpu.make_async_remote_copy(
+            src_ref=src, dst_ref=src, send_sem=sems[0].at[k], recv_sem=sems[1].at[k],
+            device_id={names[dim]: goal}, device_id_type=MESH,
+        )
+
+    def weight_block(along_y, along_z, kind, chunk):
+        first = (along_z * 4 + along_y) * 128 + 64 * kind
+        cols = (slice(0, 2 * UNITS), slice(2 * UNITS, 3 * UNITS))[chunk]
+        return wall.at[pl.ds(pl.multiple_of(first, 64), 64), cols]
+
+    def first_ring(chunk, kind, what):
+        def ref_at(i):
+            return weight_block(i, z, 0, chunk) if kind == 0 else weight_block(y, i, 1, chunk)
+
+        return ring_copy((wsend, wrecv), (chunk * 2 + kind) * 15 + what, what, ref_at, kind)
+
+    def second_ring(chunk, kind, piece, what):
+        other = (at[kind], behind[kind], ahead[kind], across[kind])[piece]
+
+        def ref_at(i):
+            if kind == 0:
+                return weight_block(other, i, 0, chunk)
+            return weight_block(i, other, 1, chunk)
+
+        k = (chunk * 2 + kind) * 15 + 3 + piece * 3 + what
+        return ring_copy((wsend, wrecv), k, what, ref_at, 1 - kind)
+
+    pl.semaphore_wait(barrier, 13)
+    for chunk in range(2):
+        for c in (loads[:2], loads[2:3])[chunk]:
+            c.wait()
+        for kind in range(2):
+            first_ring(chunk, kind, 0).start()
+            first_ring(chunk, kind, 1).start()
+
+    vf[...] = vals[...].astype(F32)
+    gf[...] = gates[...].astype(F32)
     for h in range(2):
-        beta, cum = gate_rows(upd[h], fade[h], boost[h], level[h, 0], bias[h, 0])
+        beta, cum = gate_rows(upd[...].astype(F32)[h : h + 1], fade[h], boost[h], level[0, h], bias[0, h])
         beta_s[h * NBLK : (h + 1) * NBLK, :] = beta
         cum_s[h * NBLK : (h + 1) * NBLK, :] = cum
 
@@ -109,12 +231,15 @@
         ins = []
         for h, n in todo:
             rows = pl.ds(pl.multiple_of(n * BLK, BLK), BLK)
-            q, k = (q1, k1) if h == 0 else (q2, k2)
+            if h == 0:
+                q, k = q1[rows, :].astype(F32), k1[rows, :].astype(F32)
+            else:
+                q, k = q2[:, rows].astype(F32).T, k2[:, rows].astype(F32).T
             ins.append(
                 block_inputs(
-                    q[rows, :],
-                    k[rows, :],
-                    vals[rows, h * BLK : (h + 1) * BLK],
+                    q,
+                    k,
+                    vf[pl.ds(2 * n * BLK + h, BLK, 2), :],
                     cum_s[pl.ds(h * NBLK + n, 1), :],
                     beta_s[pl.ds(h * NBLK + n, 1), :],
                 )
@@ -132,7 +257,16 @@
             keep_s[pl.ds(h * NBLK + n, 1), :] = i["keep"]
         return carry
 
-    lax.fori_loop(0, NBLK // 2, parts, 0)
+    lax.fori_loop(0, 2, parts, 0)
+    for kind in range(2):
+        first_ring(0, kind, 0).wait_recv()
+        first_ring(0, kind, 2).start()
+        second_ring(0, kind, 0, 0).start()
+        second_ring(0, kind, 0, 1).start()
+    lax.fori_loop(2, NBLK // 2, parts, 0)
+    for kind in range(2):
+        first_ring(1, kind, 0).wait_recv()
+        first_ring(1, kind, 2).start()
 
     def eye(dk):
         return (
@@ -162,139 +296,109 @@
         for dk in (128, 64)
     )
     (s1, g1), (s2, g2) = lax.fori_loop(0, NBLK, chain, start)
-    pay[0:128, :] = (s1[:, BLK:] - eye(128) * g1).astype(BF16)
-    pay[128:256, :] = s1[:, :BLK].astype(BF16)
-    pay[256:320, :] = s2[:, :BLK].astype(BF16)
-    row = lax.broadcasted_iota(jnp.int32, (64, 64), 0)
-    hi1, hi2 = g1.astype(BF16).astype(F32), g2.astype(BF16).astype(F32)
-    scal = jnp.where(row == 0, hi1[:, :64], 0.0)
-    scal = scal + jnp.where(row == 1, (g1 - hi1)[:, :64], 0.0)
-    scal = scal + jnp.where(row == 2, hi2[:, :64], 0.0)
-    scal = scal + jnp.where(row == 3, (g2 - hi2)[:, :64], 0.0)
-    d2 = s2[:, BLK:] - eye(64) * g2[:, :64]
-    pay[320:384, :] = jnp.concatenate([d2, scal], axis=1).astype(BF16)
-
-
-def local_recurrence(q1, k1, q2, k2, vals, upd, fade, boost, level, bias):
-    vm = pl.BlockSpec(memory_space=pltpu.VMEM)
-    sm = pl.BlockSpec(memory_space=pltpu.SMEM)
-    return pl.pallas_call(
-        local_kernel,
-        out_shape=(
-            jax.ShapeDtypeStruct((1024, 128), BF16),
-            jax.ShapeDtypeStruct((1024, 64), BF16),
-            jax.ShapeDtypeStruct((1024, 128), F32),
-            jax.ShapeDtypeStruct((1024, 128), F32),
-            jax.ShapeDtypeStruct((384, 128), BF16),
-        ),
-        in_specs=[vm] * 8 + [sm] * 2,
-        out_specs=[vm] * 5,
-        scratch_shapes=[
-            pltpu.VMEM((2 * NBLK, BLK), F32),
-            pltpu.VMEM((2 * NBLK, BLK), F32),
-            pltpu.VMEM((2 * NBLK, BLK), F32),
-            pltpu.VMEM((NBLK, 256, 128), BF16),
-            pltpu.VMEM((NBLK, 192, 64), BF16),
-            pltpu.VMEM((NBLK, BLK, BLK), F32),
-            pltpu.VMEM((NBLK, BLK, BLK), F32),
-            pltpu.VMEM((NBLK, 128, BLK), F32),
-            pltpu.VMEM((NBLK, 64, BLK), F32),
-        ],
-        cost_estimate=pl.CostEstimate(
-            flops=2_000_000_000, bytes_accessed=4_000_000, transcendentals=1_000_000
-        ),
-    )(q1, k1, q2, k2, vals, upd, fade, boost, level, bias)
-
-
-def split_pay(pay):
-    p = pay.astype(F32)
-    g1 = p[320, 64] + p[321, 64]
-    g2 = p[322, 64] + p[323, 64]
-    return (p[:128], p[128:256], g1), (p[320:, :64], p[256:320], g2)
-
-
-def join_pay(one, two):
-    (d1, a1, g1), (d2, a2, g2) = one, two
-    hi1, hi2 = lax.reduce_precision(g1, 8, 7), lax.reduce_precision(g2, 8, 7)
-    scal = jnp.stack([hi1, g1 - hi1, hi2, g2 - hi2])
-    scal = jnp.pad(jnp.broadcast_to(scal[:, None], (4, 64)), ((0, 60), (0, 0)))
-    low = jnp.concatenate([d2, scal], axis=1)
-    return jnp.concatenate([d1, a1, a2, low], axis=0).astype(BF16)
-
-
-def after(earlier, later):
-    d0, a0, g0 = earlier
-    d1, a1, g1 = later
-    return (g1 * d0 + g0 * d1 + mm(d1, d0), g1 * a0 + a1 + mm(d1, a0), g0 * g1)
-
-
-def applied(later, state):
-    d, a, g = later
-    return g * state + a + mm(d, state)
-
-
-def incoming_states(pay):
-    y, z = lax.axis_index("sp_1"), lax.axis_index("sp_0")
-    row = lax.all_gather(pay, "sp_1")
-    members = [split_pay(row[i]) for i in range(4)]
-    whole = members[0]
-    for m in members[1:]:
-        whole = tuple(after(e, l) for e, l in zip(whole, m))
-    rows = lax.all_gather(join_pay(*whole), "sp_0")
-    states = [jnp.zeros((128, 128), F32), jnp.zeros((64, 128), F32)]
-    for i in range(3):
-        states = [
-            jnp.where(i < z, applied(m, s), s) for m, s in zip(split_pay(rows[i]), states)
-        ]
-    for i in range(3):
-        states = [jnp.where(i < y, applied(m, s), s) for m, s in zip(members[i], states)]
-    return states
-
-
-def finished_head(local, reads, state, gate_cols, coef):
-    out = local + mm(reads, state)
-    scaled = out * lax.rsqrt(jnp.mean(out * out, axis=-1, keepdims=True) + EPSILON) * coef
-    return (scaled * jax.nn.silu(gate_cols.astype(F32))).astype(BF16)
-
-
-MESH = pl.DeviceIdType.MESH
-WIDTH = 2048
-UNITS = 768
-
-
-def ring_places():
-    me = lax.axis_index("tp")
-    x, core = me // 2, me % 2
-    right = ((x + 1) % 4) * 2 + core
-    left = ((x + 3) % 4) * 2 + core
-    far = ((x + 2) % 4) * 2 + core
-    return me, x, core, x * 2 + 1 - core, right, left, far
-
-
-def mixer_kernel(
-    normed, skip, taps, weights,
-    out,
-    feat, wgu, wdn, low, hid, acc, d2d_out, d2d_in, far_out, msg_r, msg_l, far_in, in_l, in_r,
-    load_sem, send_sem, recv_sem,
-):
-    me, x, core, mate, right, left, far = ring_places()
-    z, y = lax.axis_index("sp_0"), lax.axis_index("sp_1")
-    place = z * 4 + y
-    after_z, after_y = ((place + 1) % 16) // 4, (place + 1) % 4
-    prior_z, prior_y = ((place + 15) % 16) // 4, (place + 15) % 4
-    to_mate, to_right, to_left = {"tp": mate}, {"tp": right}, {"tp": left}
-    to_next = {"sp_0": after_z, "sp_1": after_y}
-    to_prior = {"sp_0": prior_z, "sp_1": prior_y}
-
-    load_gu = pltpu.make_async_copy(weights.at[:, 0 : 2 * UNITS], wgu, load_sem.at[0])
-    load_dn = pltpu.make_async_copy(weights.at[:, 2 * UNITS :], wdn, load_sem.at[1])
-    load_gu.start()
-    load_dn.start()
-
-    barrier = pltpu.get_barrier_semaphore()
-    for peer in (to_mate, to_right, to_left, to_next, to_prior):
-        pl.semaphore_signal(barrier, inc=1, device_id=peer, device_id_type=MESH)
-    pl.semaphore_wait(barrier, 5)
+    write_maps(
+        pays,
+        y,
+        (s1[:, BLK:] - eye(128) * g1, s1[:, :BLK], g1[:, :1]),
+        (s2[:, BLK:] - eye(64) * g2[:, :64], s2[:, :BLK], g2[:, :1]),
+    )
+
+    def exchange(buf, dim, what):
+        sems = (send_sem, recv_sem)
+        return ring_copy(sems, 22 + dim * 3 + what, what, lambda i: buf.at[i], dim)
+
+    exchange(pays, 0, 0).start()
+    exchange(pays, 0, 1).start()
+    for kind in range(2):
+        second_ring(0, kind, 0, 0).wait_recv()
+    exchange(pays, 0, 0).wait_recv()
+    exchange(pays, 0, 2).start()
+    for kind in range(2):
+        second_ring(0, kind, 0, 2).start()
+    exchange(pays, 0, 1).wait_recv()
+    exchange(pays, 0, 2).wait_recv()
+    whole = read_maps(pays, 0)
+    whole = tuple((d.astype(F32), a, g) for d, a, g in whole)
+    for i in range(1, 4):
+        whole = tuple(after(e, l) for e, l in zip(whole, read_maps(pays, i)))
+    write_maps(row_pays, z, *whole)
+    exchange(row_pays, 1, 0).start()
+    exchange(row_pays, 1, 1).start()
+    exchange(row_pays, 1, 0).wait_recv()
+    exchange(row_pays, 1, 2).start()
+    for kind in range(2):
+        first_ring(0, kind, 1).wait_recv()
+        first_ring(0, kind, 2).wait_recv()
+        for piece in (1, 2, 3):
+            second_ring(0, kind, piece, 0).start()
+            second_ring(0, kind, piece, 1).start()
+    exchange(row_pays, 1, 1).wait_recv()
+    exchange(row_pays, 1, 2).wait_recv()
+
+    states = [jnp.zeros((128, BLK), F32), jnp.zeros((64, BLK), F32)]
+    for buf, limit in ((row_pays, z), (pays, y)):
+        for i in range(3):
+            moved = [
+                s * g + a + mm(d, s) for (d, a, g), s in zip(read_maps(buf, i), states)
+            ]
+            states = [jnp.where(i < limit, m, s) for m, s in zip(moved, states)]
+    states = [s.astype(BF16) for s in states]
+
+    order = (far, far + 1 - 2 * core, right, right + 1 - 2 * core, left, left + 1 - 2 * core, mate)
+
+    def finish(n):
+        rows = pl.ds(pl.multiple_of(n * BLK, BLK), BLK)
+        for h in range(2):
+            o, r = ((o1, r1), (o2, r2))[h]
+            head = o[rows, :] + mm(r[rows, :], states[h])
+            scale = lax.rsqrt(jnp.mean(head * head, axis=-1, keepdims=True) + EPSILON)
+            g = gf[pl.ds(2 * n * BLK + h, BLK, 2), :]
+            made = head * scale * norm_coef[...] * (g / (1.0 + jnp.exp(-g)))
+            heads[n, :, h * BLK : (h + 1) * BLK] = made.astype(BF16)
+
+    def hand_out(k):
+        return pltpu.make_async_remote_copy(
+            src_ref=heads.at[order[k]], dst_ref=arrived.at[me],
+            send_sem=send_sem.at[28 + k], recv_sem=recv_sem.at[28 + k],
+            device_id={"tp": order[k]}, device_id_type=MESH,
+        )
+
+    for k in range(7):
+        finish(order[k])
+        hand_out(k).start()
+    finish(me)
+    arrived[me] = heads[me]
+    skip[...] = hidden[...].astype(F32)
+    loads[3].wait()
+
+    def emit(pair):
+        firsts = [arrived[2 * pair + i] for i in range(2)]
+        one = jnp.concatenate([f[:, :BLK] for f in firsts], axis=1)
+        two = jnp.concatenate([f[:, BLK:] for f in firsts], axis=1)
+        upper = pl.ds(pl.multiple_of(pair * 256, 256), 256)
+        lower = pl.ds(pl.multiple_of(pair * 256 + 1024, 256), 256)
+
+        def tile(j, carry):
+            cols = pl.ds(pl.multiple_of(j * 512, 512), 512)
+            skip[:, cols] += mm(one, emit_w[upper, cols]) + mm(two, emit_w[lower, cols])
+            return carry
+
+        lax.fori_loop(0, 4, tile, 0)
+
+    hand_out(6).wait_recv()
+    emit(x)
+    hand_out(2).wait_recv()
+    hand_out(3).wait_recv()
+    emit((x + 3) % 4)
+    hand_out(4).wait_recv()
+    hand_out(5).wait_recv()
+    emit((x + 1) % 4)
+    hand_out(0).wait_recv()
+    hand_out(1).wait_recv()
+    emit((x + 2) % 4)
+    full = skip[...]
+    norm = lax.rsqrt(jnp.mean(full * full, axis=-1, keepdims=True) + EPSILON)
+    normed[...] = (full * norm * chan_coef[...]).astype(BF16)
 
     def send(k, src, dst, peer):
         return pltpu.make_async_remote_copy(
@@ -317,6 +421,15 @@
     for c in own:
         c.start()
     a_right, b_left, b_right, a_left = own
+    for kind in range(2):
+        for piece in (1, 2, 3):
+            second_ring(0, kind, piece, 0).wait_recv()
+            second_ring(0, kind, piece, 2).start()
+        first_ring(1, kind, 1).wait_recv()
+        first_ring(1, kind, 2).wait_recv()
+        for piece in range(4):
+            second_ring(1, kind, piece, 0).start()
+            second_ring(1, kind, piece, 1).start()
     fwd_a = send(5, shard(left, 0, 64), shard(left, 0, 64), to_right)
     fwd_b = send(6, shard(right, 64, 64), shard(right, 64, 64), to_left)
     mate_l = send(7, shard(left), shard(left), to_mate)
@@ -334,7 +447,7 @@
 
         def tile(j, carry):
             cols = pl.ds(pl.multiple_of(j * 256, 256), 256)
-            low[put, cols] = mm(feat[rows, :], wgu[:, cols]).astype(BF16)
+            low[put, cols] = mm(feat[rows, :], wall[:, cols]).astype(BF16)
             return carry
 
         lax.fori_loop(0, 6, tile, 0)
@@ -343,17 +456,26 @@
         def _():
             halo.start()
 
-    load_gu.wait()
-    own_mate.wait_recv()
-    gate_up(x)
     a_right.wait_recv()
     fwd_a.start()
     b_left.wait_recv()
     fwd_b.start()
+    for kind in range(2):
+        second_ring(0, kind, 0, 1).wait_recv()
+        second_ring(0, kind, 0, 2).wait_recv()
+        for piece in (1, 2, 3):
+            second_ring(0, kind, piece, 1).wait_recv()
+            second_ring(0, kind, piece, 2).wait_recv()
+    own_mate.wait_recv()
+    gate_up(x)
     b_right.wait_recv()
     mate_l.start()
     a_left.wait_recv()
     mate_r.start()
+    for kind in range(2):
+        for piece in range(4):
+            second_ring(1, kind, piece, 0).wait_recv()
+            second_ring(1, kind, piece, 2).start()
     mate_r.wait_recv()
     gate_up((x + 1) % 4)
     mate_l.wait_recv()
@@ -365,7 +487,10 @@
     mate_fa.wait_recv()
     mate_fb.wait_recv()
     gate_up((x + 2) % 4)
-    load_dn.wait()
+    for kind in range(2):
+        for piece in range(4):
+            second_ring(1, kind, piece, 1).wait_recv()
+            second_ring(1, kind, piece, 2).wait_recv()
     halo.wait_recv()
 
     @pl.when(place == 0)
@@ -395,7 +520,7 @@
         def tile(j, carry):
             span = pl.ds(pl.multiple_of(j * 256, 256), 256)
             both = jnp.concatenate([hid[mine, :], hid[other, :]], axis=0)
-            made = mm_nt(both, wdn[span, :])
+            made = mm_nt(both, wall[span, 2 * UNITS :])
             acc[k, :, span] = made[:128]
             d2d_out[k, :, span] = made[128:].astype(BF16)
             return carry
@@ -446,41 +571,68 @@
         c.wait_send()
     for c in (d_far, d_right, d_left, d_own, far_a, far_b, r_b, r_a, l_a, l_b):
         c.wait_send()
-
-
-def channel_mixer(normed, skip, taps, weights):
+    for dim, buf in ((0, pays), (1, row_pays)):
+        for what in range(3):
+            exchange(buf, dim, what).wait_send()
+    for k in range(7):
+        hand_out(k).wait_send()
+    for chunk in range(2):
+        for kind in range(2):
+            for what in range(3):
+                first_ring(chunk, kind, what).wait_send()
+                for piece in range(4):
+                    second_ring(chunk, kind, piece, what).wait_send()
+
+
+def whole_layer(*args):
     vm = pl.BlockSpec(memory_space=pltpu.VMEM)
+    sm = pl.BlockSpec(memory_space=pltpu.SMEM)
+    hbm = pl.BlockSpec(memory_space=pl.ANY)
+    block = [(128, WIDTH)] * 6
     return pl.pallas_call(
-        mixer_kernel,
+        layer_kernel,
         out_shape=jax.ShapeDtypeStruct((128, WIDTH), BF16),
-        in_specs=[vm, vm, vm, pl.BlockSpec(memory_space=pl.ANY)],
+        in_specs=[vm] * 9 + [sm] * 2 + [vm, hbm, vm, vm, hbm, hbm, hbm, vm],
         out_specs=vm,
         scratch_shapes=[
+            *[pltpu.VMEM((2 * NBLK, BLK), F32)] * 3,
+            pltpu.VMEM((NBLK, 256, 128), BF16),
+            pltpu.VMEM((NBLK, 192, 64), BF16),
+            pltpu.VMEM((NBLK, BLK, BLK), F32),
+            pltpu.VMEM((NBLK, BLK, BLK), F32),
+            pltpu.VMEM((NBLK, 128, BLK), F32),
+            pltpu.VMEM((NBLK, 64, BLK), F32),
+            pltpu.VMEM((2048, BLK), F32),
+            pltpu.VMEM((2048, BLK), F32),
+            pltpu.VMEM((1024, 128), BF16),
+            pltpu.VMEM((1024, 64), BF16),
+            pltpu.VMEM((1024, BLK), F32),
+            pltpu.VMEM((1024, BLK), F32),
+            pltpu.VMEM((4, 384, 128), BF16),
+            pltpu.VMEM((4, 384, 128), BF16),
+            pltpu.VMEM((8, 128, 256), BF16),
+            pltpu.VMEM((8, 128, 256), BF16),
+            pltpu.VMEM((WIDTH, WIDTH), BF16),
+            pltpu.VMEM((128, WIDTH), F32),
+            pltpu.VMEM((128, WIDTH), BF16),
+            pltpu.VMEM((WIDTH, 3 * UNITS), BF16),
             pltpu.VMEM((1024, WIDTH), BF16),
-            pltpu.VMEM((WIDTH, 2 * UNITS), BF16),
-            pltpu.VMEM((WIDTH, UNITS), BF16),
             pltpu.VMEM((1040, 2 * UNITS), BF16),
             pltpu.VMEM((256, UNITS), BF16),
             pltpu.VMEM((4, 128, WIDTH), F32),
             pltpu.VMEM((4, 128, WIDTH), BF16),
             pltpu.VMEM((4, 128, WIDTH), BF16),
-            pltpu.VMEM((128, WIDTH), BF16),
-            pltpu.VMEM((128, WIDTH), BF16),
-            pltpu.VMEM((128, WIDTH), BF16),
-            pltpu.VMEM((128, WIDTH), BF16),
-            pltpu.VMEM((128, WIDTH), BF16),
-            pltpu.VMEM((128, WIDTH), BF16),
-            pltpu.SemaphoreType.DMA((2,)),
-            pltpu.SemaphoreType.DMA((22,)),
-            pltpu.SemaphoreType.DMA((22,)),
+            *[pltpu.VMEM(b, BF16) for b in block],
+            pltpu.SemaphoreType.DMA((4,)),
+            pltpu.SemaphoreType.DMA((35,)),
+            pltpu.SemaphoreType.DMA((35,)),
+            pltpu.SemaphoreType.DMA((60,)),
+            pltpu.SemaphoreType.DMA((60,)),
         ],
         compiler_params=pltpu.CompilerParams(
-            collective_id=1, has_side_effects=True, vmem_limit_bytes=60 * 1024 * 1024
+            collective_id=1, has_side_effects=True, vmem_limit_bytes=62 * 1024 * 1024
         ),
-        cost_estimate=pl.CostEstimate(
-            flops=10_000_000_000, bytes_accessed=12_000_000, transcendentals=1_000_000
-        ),
-    )(normed, skip, taps, weights)
+    )(*args)
 
 
 def per_device(
@@ -504,46 +656,27 @@
     timewise_convolve_tapvalues,
     narrowing_map_weights_in,
 ):
-    gathered = lax.all_gather(
-        jnp.concatenate(
-            [switching_channel_map, broadening_channel_map, narrowing_map_weights_in], axis=1
-        ),
-        SP,
-        axis=0,
-        tiled=True,
-    )
-    vals = stored_vectors_both.reshape(-1, 256)
-    r1, r2, o1, o2, pay = local_recurrence(
+    return whole_layer(
         former_request_vectors,
         former_match_vectors,
-        latter_request_vectors,
-        latter_match_vectors,
-        vals,
-        update_level_before_squash,
+        latter_request_vectors.T,
+        latter_match_vectors.T,
+        stored_vectors_both.reshape(-1, 128),
+        closing_valve_operands.reshape(-1, 128),
+        update_level_before_squash.reshape(2, -1),
         fading_data_input,
         sparse_fading_boost,
-        unitwise_fading_loglevel,
-        fading_constant_term,
+        unitwise_fading_loglevel.reshape(1, 2),
+        fading_constant_term.reshape(1, 2),
+        unitwise_normalizer_coef.reshape(1, -1),
+        emission_map_weights,
+        channel_normalizer_coef.reshape(1, -1),
+        arriving_hidden_state,
+        switching_channel_map,
+        broadening_channel_map,
+        narrowing_map_weights_in,
+        timewise_convolve_tapvalues,
     )
-    s1, s2 = incoming_states(pay)
-    linear_attend = jnp.stack(
-        [
-            finished_head(o1, r1, s1, closing_valve_operands[:, 0], unitwise_normalizer_coef),
-            finished_head(o2, r2, s2, closing_valve_operands[:, 1], unitwise_normalizer_coef),
-        ],
-        axis=1,
-    )
-    arrived = lax.all_to_all(linear_attend, "tp", split_axis=0, concat_axis=2, tiled=True)
-    row_count = arrived.shape[0]
-    skip_stream = arriving_hidden_state.astype(jnp.float32) + jnp.dot(
-        arrived.reshape(row_count, -1), emission_map_weights, preferred_element_type=jnp.float32
-    )
-    normed = (
-        skip_stream
-        * lax.rsqrt(jnp.mean(skip_stream * skip_stream, axis=-1, keepdims=True) + EPSILON)
-        * channel_normalizer_coef
-    ).astype(jnp.bfloat16)
-    return channel_mixer(normed, skip_stream, timewise_convolve_tapvalues, gathered)
 
 
 def solution(mesh):

time: 187 us -> 110 us (0.59)
  blocking collectives: 44.3 us -> 0 us
  Pallas kernels: 73.8 us -> 108 us
  between operations: 33.1 us -> 0.01 us
  local copies, waits for them, and re-layouts: 16.2 us -> 1.88 us
  matrix products: 13.3 us -> 0 us
  other arithmetic: 5.16 us -> 0 us
    pallas_call x2 -> x1, Pallas kernels: 73.8 us -> 108 us  [whole_layer(): pl.pallas_call(layer_kernel, out_shape=jax.ShapeDtypeStruct((128, WIDTH),...]
    all_gather x2 -> x0, blocking collectives: 26.9 us -> none  [the longest x1 14.1 us: incoming_states(): rows = lax.all_gather(join_pay(*whole), 'sp_0')]
    all_to_all x1 -> x0, blocking collectives: 17.4 us -> none  [per_device(): lax.all_to_all(linear_attend, 'tp', split_axis=0, concat_axis=2, tiled=True)]
    dot_general x25 -> x0, matrix products: 13.3 us -> none  [the longest x24 8.54 us: mm(): return jnp.dot(a.astype(BF16), b.astype(BF16), preferred_element_type=F32)]
    unnamed x25 -> x1, local copies, waits for them, and re-layouts: 11.2 us -> 1.88 us
    slice x6 -> x0, local copies, waits for them, and re-layouts: 4.03 us -> none  [the longest x5 3.3 us: split_pay(): g1 = p[320, 64] + p[321, 64]]
    concatenate x3 -> x0, other arithmetic: 2.06 us -> none  [the longest x1 1.97 us: per_device(): jnp.concatenate([switching_channel_map, broadening_channel_map, narrowing...]
  transfers between devices with their start and end apart: 1 -> 0, of which waited for: 0 -> 0; matrix products, arithmetic and copies ran while one was open for 17% -> 0% of each run, Pallas kernels for 7% -> 0%
where the time goes in v2:
time: 110 us
  Pallas kernels  108 us (98%)
  local copies, waits for them, and re-layouts  1.88 us (2%)
    pallas_call x1, Pallas kernels, whole_layer(): pl.pallas_call(layer_kernel, out_shape=jax.ShapeDtypeStruct((128, WIDTH),...  108 us

profile of v2, /device:TPU:1, one launch (start us, length us, event | category | flops | bytes accessed | tf_op | source)
XLA Modules:
  0.0 110.1 jit_solution(6354334392222538181)
XLA Ops:
  0.0 108.2 %shard_map.181 = bf16[128,2048]{1,0:T(8,128)(2,1)} custom-call(bf16[1024,128]{1,0:T(8,128)(2,1)} %q1.1, bf16[1024,128]{1,0:T(8,128)(2,1)} %k1.1, bf16[64,1024]{1,0:T(8,128)(2,1)} %bitcast.11, bf16[64,1024]{1,0:T(8,128)(2,1)} %bitcast.12, bf16[2048,128]{1,0:T(8,128)(2,1)} %bitcast.9, bf16[2048,128]{1,0:T(8,128)(2,1)} %bitcast.10, bf16[2,1024]{1,0:T(2,128)(2,1)} %bitcast.14, ...), custom_call_target="tpu_custom_call" | custom-call | tf_op jit(solution)/shard_map/pallas_call | solution.py:592
  108.2 1.9 %copy.21 = bf16[128,2048]{1,0:T(8,128)(2,1)} copy(bf16[128,2048]{1,0:T(8,128)(2,1)} %shard_map.181) | data formatting | bytes 1048576

commit v3 on v2

--- a/solution.py
+++ b/solution.py
@@ -140,11 +140,12 @@
 
 
 def layer_kernel(
-    q1, k1, q2, k2, vals, gates, upd, fade, boost, level, bias, norm_coef,
-    emission, chan_coef, hidden, w_gate, w_up, w_down, taps,
+    q1_in, k1_in, q2_in, k2_in, vals_in, gates_in, upd, fade, boost, level, bias, norm_coef,
+    emission, chan_coef, hidden_in, w_gate, w_up, w_down, taps,
     out,
     beta_s, cum_s, keep_s, qd1, qd2, loc1, loc2, add1, add2, vf, gf, r1, r2, o1, o2,
-    pays, row_pays, heads, arrived, emit_w, skip, normed, wall,
+    pays, row_pays, heads, arrived, emit_w, skip, normed, wall, wdt, wd_own,
+    q1, k1, q2, k2, vals, gates, hidden,
     feat, low, hid, acc, d2d_out, d2d_in, far_out, msg_r, msg_l, far_in, in_l, in_r,
     load_sem, send_sem, recv_sem, wsend, wrecv,
 ):
@@ -161,11 +162,17 @@
     loads = [
         pltpu.make_async_copy(w_gate, wall.at[home, 0:UNITS], load_sem.at[0]),
         pltpu.make_async_copy(w_up, wall.at[home, UNITS : 2 * UNITS], load_sem.at[1]),
-        pltpu.make_async_copy(w_down, wall.at[home, 2 * UNITS :], load_sem.at[2]),
+        pltpu.make_async_copy(w_down, wd_own, load_sem.at[2]),
         pltpu.make_async_copy(emission, emit_w, load_sem.at[3]),
     ]
-    for c in loads:
+    for c in loads[:3]:
         c.start()
+    given = (q1_in, k1_in, q2_in, k2_in, vals_in, gates_in, hidden_in)
+    taken = (q1, k1, q2, k2, vals, gates, hidden)
+    for i in range(7):
+        loads.append(pltpu.make_async_copy(given[i], taken[i], load_sem.at[4 + i]))
+        loads[-1].start()
+    loads[3].start()
 
     step = 1 - 2 * core
     at = (y, z)
@@ -191,8 +198,9 @@
 
     def weight_block(along_y, along_z, kind, chunk):
         first = (along_z * 4 + along_y) * 128 + 64 * kind
-        cols = (slice(0, 2 * UNITS), slice(2 * UNITS, 3 * UNITS))[chunk]
-        return wall.at[pl.ds(pl.multiple_of(first, 64), 64), cols]
+        if chunk == 1:
+            return wdt.at[along_z * 4 + along_y, pl.ds(384 * kind, 384), :]
+        return wall.at[pl.ds(pl.multiple_of(first, 64), 64), :]
 
     def first_ring(chunk, kind, what):
         def ref_at(i):
@@ -215,10 +223,16 @@
     for chunk in range(2):
         for c in (loads[:2], loads[2:3])[chunk]:
             c.wait()
+        if chunk == 1:
+            for i in range(6):
+                piece = slice(i * BLK, (i + 1) * BLK)
+                wdt[place, piece, :] = wd_own[:, piece].astype(F32).T.astype(BF16)
         for kind in range(2):
             first_ring(chunk, kind, 0).start()
             first_ring(chunk, kind, 1).start()
 
+    for c in loads[4:]:
+        c.wait()
     vf[...] = vals[...].astype(F32)
     gf[...] = gates[...].astype(F32)
     for h in range(2):
@@ -257,13 +271,13 @@
             keep_s[pl.ds(h * NBLK + n, 1), :] = i["keep"]
         return carry
 
-    lax.fori_loop(0, 2, parts, 0)
+    lax.fori_loop(0, 3, parts, 0)
     for kind in range(2):
         first_ring(0, kind, 0).wait_recv()
         first_ring(0, kind, 2).start()
         second_ring(0, kind, 0, 0).start()
         second_ring(0, kind, 0, 1).start()
-    lax.fori_loop(2, NBLK // 2, parts, 0)
+    lax.fori_loop(3, NBLK // 2, parts, 0)
     for kind in range(2):
         first_ring(1, kind, 0).wait_recv()
         first_ring(1, kind, 2).start()
@@ -309,12 +323,19 @@
 
     exchange(pays, 0, 0).start()
     exchange(pays, 0, 1).start()
-    for kind in range(2):
-        second_ring(0, kind, 0, 0).wait_recv()
+    first_ring(0, 0, 1).wait_recv()
+    first_ring(0, 0, 2).wait_recv()
+    for piece in (1,):
+        second_ring(0, 0, piece, 0).start()
+        second_ring(0, 0, piece, 1).start()
     exchange(pays, 0, 0).wait_recv()
     exchange(pays, 0, 2).start()
-    for kind in range(2):
-        second_ring(0, kind, 0, 2).start()
+    for piece in (0,):
+        second_ring(0, 0, piece, 0).wait_recv()
+        second_ring(0, 0, piece, 2).start()
+    for piece in (0,):
+        second_ring(0, 1, piece, 0).wait_recv()
+        second_ring(0, 1, piece, 2).start()
     exchange(pays, 0, 1).wait_recv()
     exchange(pays, 0, 2).wait_recv()
     whole = read_maps(pays, 0)
@@ -324,14 +345,16 @@
     write_maps(row_pays, z, *whole)
     exchange(row_pays, 1, 0).start()
     exchange(row_pays, 1, 1).start()
+    first_ring(0, 1, 1).wait_recv()
+    first_ring(0, 1, 2).wait_recv()
+    for piece in (1, 2, 3):
+        second_ring(0, 1, piece, 0).start()
+        second_ring(0, 1, piece, 1).start()
     exchange(row_pays, 1, 0).wait_recv()
     exchange(row_pays, 1, 2).start()
-    for kind in range(2):
-        first_ring(0, kind, 1).wait_recv()
-        first_ring(0, kind, 2).wait_recv()
-        for piece in (1, 2, 3):
-            second_ring(0, kind, piece, 0).start()
-            second_ring(0, kind, piece, 1).start()
+    for piece in (2, 3):
+        second_ring(0, 0, piece, 0).start()
+        second_ring(0, 0, piece, 1).start()
     exchange(row_pays, 1, 1).wait_recv()
     exchange(row_pays, 1, 2).wait_recv()
 
@@ -353,7 +376,7 @@
             head = o[rows, :] + mm(r[rows, :], states[h])
             scale = lax.rsqrt(jnp.mean(head * head, axis=-1, keepdims=True) + EPSILON)
             g = gf[pl.ds(2 * n * BLK + h, BLK, 2), :]
-            made = head * scale * norm_coef[...] * (g / (1.0 + jnp.exp(-g)))
+            made = head * scale * norm_coef[...] * (0.5 * g * (1.0 + jnp.tanh(0.5 * g)))
             heads[n, :, h * BLK : (h + 1) * BLK] = made.astype(BF16)
 
     def hand_out(k):
@@ -363,11 +386,17 @@
             device_id={"tp": order[k]}, device_id_type=MESH,
         )
 
+    for piece in (1,):
+        second_ring(0, 0, piece, 0).wait_recv()
+        second_ring(0, 0, piece, 2).start()
     for k in range(7):
         finish(order[k])
         hand_out(k).start()
     finish(me)
     arrived[me] = heads[me]
+    for piece in (1,):
+        second_ring(0, 1, piece, 0).wait_recv()
+        second_ring(0, 1, piece, 2).start()
     skip[...] = hidden[...].astype(F32)
     loads[3].wait()
 
@@ -383,16 +412,38 @@
             skip[:, cols] += mm(one, emit_w[upper, cols]) + mm(two, emit_w[lower, cols])
             return carry
 
-        lax.fori_loop(0, 4, tile, 0)
+        lax.fori_loop(0, 4, tile, 0, unroll=2)
 
     hand_out(6).wait_recv()
     emit(x)
+    for piece in (2,):
+        second_ring(0, 1, piece, 0).wait_recv()
+        second_ring(0, 1, piece, 2).start()
+    for piece in (2,):
+        second_ring(0, 0, piece, 0).wait_recv()
+        second_ring(0, 0, piece, 2).start()
     hand_out(2).wait_recv()
     hand_out(3).wait_recv()
     emit((x + 3) % 4)
+    for piece in (3,):
+        second_ring(0, 1, piece, 0).wait_recv()
+        second_ring(0, 1, piece, 2).start()
+    for piece in (3,):
+        second_ring(0, 0, piece, 0).wait_recv()
+        second_ring(0, 0, piece, 2).start()
     hand_out(4).wait_recv()
     hand_out(5).wait_recv()
     emit((x + 1) % 4)
+    first_ring(1, 0, 1).wait_recv()
+    first_ring(1, 0, 2).wait_recv()
+    first_ring(1, 1, 1).wait_recv()
+    first_ring(1, 1, 2).wait_recv()
+    for piece in range(4):
+        second_ring(1, 0, piece, 0).start()
+        second_ring(1, 0, piece, 1).start()
+    for piece in range(4):
+        second_ring(1, 1, piece, 0).start()
+        second_ring(1, 1, piece, 1).start()
     hand_out(0).wait_recv()
     hand_out(1).wait_recv()
     emit((x + 2) % 4)
@@ -420,46 +471,104 @@
     own_mate.start()
     for c in own:
         c.start()
-    a_right, b_left, b_right, a_left = own
-    for kind in range(2):
-        for piece in (1, 2, 3):
-            second_ring(0, kind, piece, 0).wait_recv()
-            second_ring(0, kind, piece, 2).start()
-        first_ring(1, kind, 1).wait_recv()
-        first_ring(1, kind, 2).wait_recv()
-        for piece in range(4):
-            second_ring(1, kind, piece, 0).start()
-            second_ring(1, kind, piece, 1).start()
+    a_right, b_left, b_right, a_left = tuple(own)
     fwd_a = send(5, shard(left, 0, 64), shard(left, 0, 64), to_right)
     fwd_b = send(6, shard(right, 64, 64), shard(right, 64, 64), to_left)
-    mate_l = send(7, shard(left), shard(left), to_mate)
-    mate_r = send(8, shard(right), shard(right), to_mate)
+    mate_la = send(7, shard(left, 0, 64), shard(left, 0, 64), to_mate)
+    mate_rb = send(8, shard(right, 64, 64), shard(right, 64, 64), to_mate)
+    mate_lb = send(35, shard(left, 64, 64), shard(left, 64, 64), to_mate)
+    mate_ra = send(36, shard(right, 0, 64), shard(right, 0, 64), to_mate)
     mate_fa = send(9, shard(far, 0, 64), shard(far, 0, 64), to_mate)
     mate_fb = send(10, shard(far, 64, 64), shard(far, 64, 64), to_mate)
-    halo_rows = low.at[pl.ds(1024, 16), :]
-    halo = send(11, halo_rows, low.at[pl.ds(0, 16), :], to_next)
+    halo = send(11, low.at[:, 1024:1032, :], low.at[:, 0:8, :], to_next)
 
     feat[pl.ds(pl.multiple_of(me * 128, 128), 128), :] = normed[...]
 
-    def gate_up(pair):
-        rows = pl.ds(pl.multiple_of(pair * 256, 256), 256)
-        put = pl.ds(pl.multiple_of(pair * 256 + 16, 16), 256)
+    def gate_up(segments, first=0, last=6):
+        count = 256 // len(segments)
+        starts = [pl.multiple_of(s, 64) for s in segments]
 
         def tile(j, carry):
             cols = pl.ds(pl.multiple_of(j * 256, 256), 256)
-            low[put, cols] = mm(feat[rows, :], wall[:, cols]).astype(BF16)
+            rows = jnp.concatenate([feat[pl.ds(s, count), :] for s in starts], axis=0)
+            made = mm(rows, wall[:, cols]).astype(BF16).astype(F32)
+            for i, s in enumerate(starts):
+                for half in range(2):
+                    low[2 * j + half, pl.ds(pl.multiple_of(s + 8, 8), count), :] = made[
+                        i * count : (i + 1) * count, half * BLK : (half + 1) * BLK
+                    ]
             return carry
 
-        lax.fori_loop(0, 6, tile, 0)
-
-        @pl.when(pair == 3)
-        def _():
-            halo.start()
-
-    a_right.wait_recv()
-    fwd_a.start()
-    b_left.wait_recv()
-    fwd_b.start()
+        lax.fori_loop(first, last, tile, 0, unroll=2 if (last - first) % 2 == 0 else 3)
+
+    def conv(pair, first, count):
+        start = pair * 256 + first
+
+        def mix(j, carry):
+            span = pl.ds(pl.multiple_of(j * BLK, BLK), BLK)
+            total = []
+            for side in range(2):
+                t = [taps[i, side : side + 1, span].astype(F32) for i in range(3)]
+                w = [low[j + 6 * side, pl.ds(start + 6 + i, count), :] for i in range(3)]
+                total.append(t[0] * w[0] + t[1] * w[1] + t[2] * w[2])
+            g, u = total
+            rows = pl.ds(pl.multiple_of(start, 64), count)
+            hid[rows, span] = (0.5 * g * (1.0 + jnp.tanh(0.5 * g)) * u).astype(BF16)
+            return carry
+
+        lax.fori_loop(0, 6, mix, 0)
+
+    wide = (slice(0, 1024), slice(1024, 2048))
+
+    def down(k, pair, sem, first=0, count=128, part=None):
+        mine = pl.ds(pl.multiple_of(pair * 256 + core * 128 + first, 64), count)
+        other = pl.ds(pl.multiple_of(pair * 256 + (1 - core) * 128 + first, 64), count)
+        kept = slice(first, first + count)
+
+        def tile(j, carry):
+            span = pl.ds(pl.multiple_of(j * 256, 256), 256)
+            both = jnp.concatenate([hid[mine, :], hid[other, :]], axis=0)
+            made = mm(both, jnp.concatenate([wdt[2 * j], wdt[2 * j + 1]], axis=1))
+            acc[k, kept, span] = made[:count]
+            d2d_out[k, kept, span] = made[count:].astype(BF16)
+            return carry
+
+        tiles, cols = ((0, 8), slice(None)) if part is None else ((4 * part, 4 * part + 4), wide[part])
+        lax.fori_loop(*tiles, tile, 0, unroll=4)
+        sent = send(sem, d2d_out.at[k, kept, cols], d2d_in.at[k, kept, cols], to_mate)
+        sent.start()
+        return sent
+
+    def pair_sum(k, kept, cols=slice(None)):
+        return acc[k, kept, cols] + d2d_in[k, kept, cols].astype(F32)
+
+    top, bottom = slice(0, 64), slice(64, 128)
+    pair_r, pair_l, pair_f = (x + 1) % 4, (x + 3) % 4, (x + 2) % 4
+    far_b = [
+        send((16, 38)[c], far_out.at[bottom, wide[c]], far_in.at[bottom, wide[c]], to_right)
+        for c in range(2)
+    ]
+    far_a = [
+        send((17, 39)[c], far_out.at[top, wide[c]], far_in.at[top, wide[c]], to_left)
+        for c in range(2)
+    ]
+    r_a = [
+        send((18, 45)[c], msg_r.at[top, wide[c]], in_l.at[top, wide[c]], to_right)
+        for c in range(2)
+    ]
+    r_b = [
+        send((19, 40)[c], msg_r.at[bottom, wide[c]], in_l.at[bottom, wide[c]], to_right)
+        for c in range(2)
+    ]
+    l_b = [
+        send((20, 46)[c], msg_l.at[bottom, wide[c]], in_r.at[bottom, wide[c]], to_left)
+        for c in range(2)
+    ]
+    l_a = [
+        send((21, 41)[c], msg_l.at[top, wide[c]], in_r.at[top, wide[c]], to_left)
+        for c in range(2)
+    ]
+
     for kind in range(2):
         second_ring(0, kind, 0, 1).wait_recv()
         second_ring(0, kind, 0, 2).wait_recv()
@@ -467,109 +576,138 @@
             second_ring(0, kind, piece, 1).wait_recv()
             second_ring(0, kind, piece, 2).wait_recv()
     own_mate.wait_recv()
-    gate_up(x)
-    b_right.wait_recv()
-    mate_l.start()
-    a_left.wait_recv()
-    mate_r.start()
+    gate_up([x * 256])
+
+    @pl.when(x == 3)
+    def _():
+        halo.start()
+
+    a_right.wait_recv()
+    fwd_a.start()
+    mate_la.start()
+    b_left.wait_recv()
+    fwd_b.start()
+    mate_rb.start()
+    mate_la.wait_recv()
+    mate_rb.wait_recv()
+    early = [pair_l * 256, pair_l * 256 + 128, pair_r * 256 + 64, pair_r * 256 + 192]
     for kind in range(2):
         for piece in range(4):
             second_ring(1, kind, piece, 0).wait_recv()
             second_ring(1, kind, piece, 2).start()
-    mate_r.wait_recv()
-    gate_up((x + 1) % 4)
-    mate_l.wait_recv()
-    gate_up((x + 3) % 4)
+    gate_up(early, 0, 4)
+    b_right.wait_recv()
+    mate_lb.start()
+    a_left.wait_recv()
+    mate_ra.start()
+    gate_up(early, 4, 6)
+    mate_lb.wait_recv()
+    mate_ra.wait_recv()
+    gate_up([pair_l * 256 + 64, pair_l * 256 + 192, pair_r * 256, pair_r * 256 + 128])
+
+    @pl.when(jnp.logical_or(x == 2, x == 0))
+    def _():
+        halo.start()
+
+    @pl.when(x == 3)
+    def _():
+        halo.wait_recv()
+
+    @pl.when(jnp.logical_and(place == 0, x == 3))
+    def _():
+        low[:, 0:8, :] = jnp.zeros((12, 8, BLK), F32)
+
+    conv(pair_r, 0, 256)
+    conv(pair_l, 64, 64)
+    conv(pair_l, 192, 64)
     fwd_a.wait_recv()
     mate_fa.start()
     fwd_b.wait_recv()
     mate_fb.start()
-    mate_fa.wait_recv()
-    mate_fb.wait_recv()
-    gate_up((x + 2) % 4)
     for kind in range(2):
         for piece in range(4):
             second_ring(1, kind, piece, 1).wait_recv()
             second_ring(1, kind, piece, 2).wait_recv()
-    halo.wait_recv()
-
-    @pl.when(place == 0)
+    d_right, d_left_b = [], []
+    for c in range(2):
+        d_right.append(down(1, pair_r, (12, 43)[c], part=c))
+        d_left_b.append(down(2, pair_l, (13, 44)[c], 64, 64, part=c))
+    mate_fa.wait_recv()
+    mate_fb.wait_recv()
+    for c in range(2):
+        gate_up([pair_f * 256], 2 * c, 2 * c + 2)
+        d_right[c].wait_recv()
+        msg_r[top, wide[c]] = pair_sum(1, top, wide[c]).astype(BF16)
+        r_a[c].start()
+        d_left_b[c].wait_recv()
+        msg_l[bottom, wide[c]] = pair_sum(2, bottom, wide[c]).astype(BF16)
+        l_b[c].start()
+    gate_up([pair_f * 256], 4, 6)
+
+    @pl.when(x == 1)
     def _():
-        low[0:16, :] = jnp.zeros((16, 2 * UNITS), BF16)
-
-    def conv(cols, pair, side):
-        rows = pl.ds(pl.multiple_of(pair * 256, 256), 272)
-        lows = low[rows, pl.ds(pl.multiple_of(cols + side * UNITS, 128), 128)].astype(F32)
-        span = pl.ds(pl.multiple_of(cols, 128), 128)
-        t = [taps[j, side : side + 1, span].astype(F32) for j in range(3)]
-        total = t[0] * pltpu.roll(lows, 2, 0) + t[1] * pltpu.roll(lows, 1, 0) + t[2] * lows
-        return total[16:]
-
-    def down(k, pair):
-        def mix(j, carry):
-            g = conv(j * 128, pair, 0)
-            u = conv(j * 128, pair, 1)
-            span = pl.ds(pl.multiple_of(j * 128, 128), 128)
-            hid[:, span] = (g / (1.0 + jnp.exp(-g)) * u).astype(BF16)
-            return carry
-
-        lax.fori_loop(0, 6, mix, 0)
-        mine = pl.ds(pl.multiple_of(core * 128, 128), 128)
-        other = pl.ds(pl.multiple_of((1 - core) * 128, 128), 128)
-
-        def tile(j, carry):
-            span = pl.ds(pl.multiple_of(j * 256, 256), 256)
-            both = jnp.concatenate([hid[mine, :], hid[other, :]], axis=0)
-            made = mm_nt(both, wall[span, 2 * UNITS :])
-            acc[k, :, span] = made[:128]
-            d2d_out[k, :, span] = made[128:].astype(BF16)
-            return carry
-
-        lax.fori_loop(0, 8, tile, 0)
-        pair_sum = send(12 + k, d2d_out.at[k], d2d_in.at[k], to_mate)
-        pair_sum.start()
-        return pair_sum
-
-    far_a = send(16, far_out.at[0:64, :], far_in.at[0:64, :], to_right)
-    far_b = send(17, far_out.at[64:128, :], far_in.at[64:128, :], to_left)
-    r_b = send(18, msg_r.at[64:128, :], in_l.at[64:128, :], to_right)
-    r_a = send(19, msg_r.at[0:64, :], in_l.at[0:64, :], to_right)
-    l_a = send(20, msg_l.at[0:64, :], in_r.at[0:64, :], to_left)
-    l_b = send(21, msg_l.at[64:128, :], in_r.at[64:128, :], to_left)
-
-    d_far = down(0, (x + 2) % 4)
-    d_right = down(1, (x + 1) % 4)
-    d_far.wait_recv()
-    far_out[...] = (acc[0] + d2d_in[0].astype(F32)).astype(BF16)
-    far_a.start()
-    far_b.start()
-    d_left = down(2, (x + 3) % 4)
-    d_right.wait_recv()
-    msg_r[64:128, :] = (acc[1, 64:128, :] + d2d_in[1, 64:128, :].astype(F32)).astype(BF16)
-    r_b.start()
-    d_left.wait_recv()
-    msg_l[0:64, :] = (acc[2, 0:64, :] + d2d_in[2, 0:64, :].astype(F32)).astype(BF16)
-    l_a.start()
-    d_own = down(3, x)
-    far_a.wait_recv()
-    msg_r[0:64, :] = (
-        acc[1, 0:64, :] + d2d_in[1, 0:64, :].astype(F32) + far_in[0:64, :].astype(F32)
-    ).astype(BF16)
-    r_a.start()
-    far_b.wait_recv()
-    msg_l[64:128, :] = (
-        acc[2, 64:128, :] + d2d_in[2, 64:128, :].astype(F32) + far_in[64:128, :].astype(F32)
-    ).astype(BF16)
-    l_b.start()
+        halo.start()
+
+    @pl.when(x == 2)
+    def _():
+        halo.wait_recv()
+
+    @pl.when(jnp.logical_and(place == 0, x == 2))
+    def _():
+        low[:, 0:8, :] = jnp.zeros((12, 8, BLK), F32)
+
+    conv(pair_f, 0, 256)
+    d_far = [down(0, pair_f, (14, 42)[c], part=c) for c in range(2)]
+    for c in range(2):
+        d_far[c].wait_recv()
+        far_out[:, wide[c]] = pair_sum(0, slice(0, 128), wide[c]).astype(BF16)
+        far_a[c].start()
+        far_b[c].start()
+
+    @pl.when(x < 2)
+    def _():
+        halo.wait_recv()
+
+    @pl.when(jnp.logical_and(place == 0, x < 2))
+    def _():
+        low[:, 0:8, :] = jnp.zeros((12, 8, BLK), F32)
+
+    conv(pair_l, 0, 64)
+    conv(pair_l, 128, 64)
+    d_left_a = down(2, pair_l, 37, 0, 64)
+    conv(x, 0, 256)
+    d_own = down(3, x, 15)
+    d_left_a.wait_recv()
+    acc[2, top, :] = pair_sum(2, top)
+    acc[1, bottom, :] = pair_sum(1, bottom)
+    for c in range(2):
+        cols = wide[c]
+        far_a[c].wait_recv()
+        msg_l[top, cols] = (acc[2, top, cols] + far_in[top, cols].astype(F32)).astype(BF16)
+        l_a[c].start()
+        far_b[c].wait_recv()
+        msg_r[bottom, cols] = (
+            acc[1, bottom, cols] + far_in[bottom, cols].astype(F32)
+        ).astype(BF16)
+        r_b[c].start()
     d_own.wait_recv()
     acc[3] = acc[3] + d2d_in[3].astype(F32) + skip[...]
-    for c in (r_b, l_a, r_a, l_b):
+    for c in (*r_a, *l_b):
         c.wait_recv()
-    out[...] = (acc[3] + in_l[...].astype(F32) + in_r[...].astype(F32)).astype(BF16)
-
-    for c in (own_mate, *own, fwd_a, fwd_b, mate_l, mate_r, mate_fa, mate_fb, halo):
+    acc[3, top, :] = acc[3, top, :] + in_l[top, :].astype(F32)
+    acc[3, bottom, :] = acc[3, bottom, :] + in_r[bottom, :].astype(F32)
+    for c in range(2):
+        cols = wide[c]
+        l_a[c].wait_recv()
+        out[top, cols] = (acc[3, top, cols] + in_r[top, cols].astype(F32)).astype(BF16)
+        r_b[c].wait_recv()
+        out[bottom, cols] = (acc[3, bottom, cols] + in_l[bottom, cols].astype(F32)).astype(BF16)
+
+    for c in (own_mate, *own, fwd_a, fwd_b, mate_la, mate_lb, mate_ra, mate_rb, mate_fa, mate_fb):
         c.wait_send()
-    for c in (d_far, d_right, d_left, d_own, far_a, far_b, r_b, r_a, l_a, l_b):
+    for c in (halo, *d_far, *d_right, d_left_a, *d_left_b, d_own, *far_a, *far_b):
+        c.wait_send()
+    for c in (*r_a, *r_b, *l_a, *l_b):
         c.wait_send()
     for dim, buf in ((0, pays), (1, row_pays)):
         for what in range(3):
@@ -592,7 +730,7 @@
     return pl.pallas_call(
         layer_kernel,
         out_shape=jax.ShapeDtypeStruct((128, WIDTH), BF16),
-        in_specs=[vm] * 9 + [sm] * 2 + [vm, hbm, vm, vm, hbm, hbm, hbm, vm],
+        in_specs=[hbm] * 6 + [vm] * 3 + [sm] * 2 + [vm, hbm, vm, hbm, hbm, hbm, hbm, vm],
         out_specs=vm,
         scratch_shapes=[
             *[pltpu.VMEM((2 * NBLK, BLK), F32)] * 3,
@@ -615,17 +753,23 @@
             pltpu.VMEM((WIDTH, WIDTH), BF16),
             pltpu.VMEM((128, WIDTH), F32),
             pltpu.VMEM((128, WIDTH), BF16),
-            pltpu.VMEM((WIDTH, 3 * UNITS), BF16),
+            pltpu.VMEM((WIDTH, 2 * UNITS), BF16),
+            pltpu.VMEM((16, UNITS, BLK), BF16),
+            pltpu.VMEM((128, UNITS), BF16),
+            *[pltpu.VMEM((1024, 128), BF16)] * 2,
+            *[pltpu.VMEM((64, 1024), BF16)] * 2,
+            *[pltpu.VMEM((2048, BLK), BF16)] * 2,
+            pltpu.VMEM((128, WIDTH), BF16),
             pltpu.VMEM((1024, WIDTH), BF16),
-            pltpu.VMEM((1040, 2 * UNITS), BF16),
-            pltpu.VMEM((256, UNITS), BF16),
+            pltpu.VMEM((12, 1032, BLK), F32),
+            pltpu.VMEM((1024, UNITS), BF16),
             pltpu.VMEM((4, 128, WIDTH), F32),
             pltpu.VMEM((4, 128, WIDTH), BF16),
             pltpu.VMEM((4, 128, WIDTH), BF16),
             *[pltpu.VMEM(b, BF16) for b in block],
-            pltpu.SemaphoreType.DMA((4,)),
-            pltpu.SemaphoreType.DMA((35,)),
-            pltpu.SemaphoreType.DMA((35,)),
+            pltpu.SemaphoreType.DMA((11,)),
+            pltpu.SemaphoreType.DMA((47,)),
+            pltpu.SemaphoreType.DMA((47,)),
             pltpu.SemaphoreType.DMA((60,)),
             pltpu.SemaphoreType.DMA((60,)),
         ],

time: 110 us -> 94.6 us (0.86)
  Pallas kernels: 108 us -> 92.5 us
    pallas_call x1, Pallas kernels: 108 us -> 92.5 us  [whole_layer(): pl.pallas_call(layer_kernel, out_shape=jax.ShapeDtypeStruct((128, WIDTH),...]
where the time goes in v3:
time: 94.6 us; the launch traced here: 94.4 us
  Pallas kernels  92.5 us (98%)
  local copies, waits for them, and re-layouts  1.88 us (2%)
    pallas_call x1, Pallas kernels, whole_layer(): pl.pallas_call(layer_kernel, out_shape=jax.ShapeDtypeStruct((128, WIDTH),...  92.5 us

profile of v3, /device:TPU:1, one launch (start us, length us, event | category | flops | bytes accessed | tf_op | source)
XLA Modules:
  0.0 94.4 jit_solution(15075280426457135656)
XLA Ops:
  0.0 92.5 %shard_map.181 = bf16[128,2048]{1,0:T(8,128)(2,1)} custom-call(bf16[1024,128]{1,0:T(8,128)(2,1)} %q1_in.1, bf16[1024,128]{1,0:T(8,128)(2,1)} %k1_in.1, bf16[64,1024]{1,0:T(8,128)(2,1)} %bitcast.11, bf16[64,1024]{1,0:T(8,128)(2,1)} %bitcast.12, bf16[2048,128]{1,0:T(8,128)(2,1)} %bitcast.9, bf16[2048,128]{1,0:T(8,128)(2,1)} %bitcast.10, ...), custom_call_target="tpu_custom_call" | custom-call | tf_op jit(solution)/shard_map/pallas_call | solution.py:730
  92.5 1.9 %copy.21 = bf16[128,2048]{1,0:T(8,128)(2,1)} copy(bf16[128,2048]{1,0:T(8,128)(2,1)} %shard_map.181) | data formatting | bytes 1048576

commit v4 on v3

--- a/solution.py
+++ b/solution.py
@@ -105,15 +105,6 @@
     return me, x, core, x * 2 + 1 - core, right, left, far
 
 
-def read_maps(pays, i):
-    low = pays[i, 320:384, :].astype(F32)
-    g1 = low[0:1, 64:65] + low[1:2, 64:65]
-    g2 = low[2:3, 64:65] + low[3:4, 64:65]
-    one = (pays[i, 0:128, :], pays[i, 128:256, :].astype(F32), g1)
-    two = (pays[i, 320:384, :][:, :64], pays[i, 256:320, :].astype(F32), g2)
-    return one, two
-
-
 def after(earlier, later):
     d0, a0, g0 = earlier
     d1, a1, g1 = later
@@ -125,18 +116,29 @@
     )
 
 
-def write_maps(pays, i, one, two):
-    (d1, a1, g1), (d2, a2, g2) = one, two
-    row = lax.broadcasted_iota(jnp.int32, (64, 64), 0)
-    hi1, hi2 = g1.astype(BF16).astype(F32), g2.astype(BF16).astype(F32)
-    scal = jnp.where(row == 0, jnp.broadcast_to(hi1, (64, 64)), 0.0)
-    scal = scal + jnp.where(row == 1, jnp.broadcast_to(g1 - hi1, (64, 64)), 0.0)
-    scal = scal + jnp.where(row == 2, jnp.broadcast_to(hi2, (64, 64)), 0.0)
-    scal = scal + jnp.where(row == 3, jnp.broadcast_to(g2 - hi2, (64, 64)), 0.0)
-    pays[i, 0:128, :] = d1.astype(BF16)
-    pays[i, 128:256, :] = a1.astype(BF16)
-    pays[i, 256:320, :] = a2.astype(BF16)
-    pays[i, 320:384, :] = jnp.concatenate([d2, scal], axis=1).astype(BF16)
+def read_map(h, buf, i):
+    if h == 0:
+        g = buf[i, 256:272, :].astype(F32)
+        return buf[i, 0:128, :], buf[i, 128:256, :].astype(F32), g[0:1, 0:1] + g[1:2, 0:1]
+    both = buf[i, 64:128, :]
+    g = both.astype(F32)
+    return both[:, :64], buf[i, 0:64, :].astype(F32), g[0:1, 64:65] + g[1:2, 64:65]
+
+
+def write_map(h, buf, i, whole):
+    d, a, g = whole
+    shape = ((16, 128), (64, 64))[h]
+    row = lax.broadcasted_iota(jnp.int32, shape, 0)
+    high = g.astype(BF16).astype(F32)
+    scal = jnp.where(row == 0, jnp.broadcast_to(high, shape), 0.0)
+    scal = scal + jnp.where(row == 1, jnp.broadcast_to(g - high, shape), 0.0)
+    if h == 0:
+        buf[i, 0:128, :] = d.astype(BF16)
+        buf[i, 128:256, :] = a.astype(BF16)
+        buf[i, 256:272, :] = scal.astype(BF16)
+    else:
+        buf[i, 0:64, :] = a.astype(BF16)
+        buf[i, 64:128, :] = jnp.concatenate([d, scal], axis=1).astype(BF16)
 
 
 def layer_kernel(
@@ -144,7 +146,7 @@
     emission, chan_coef, hidden_in, w_gate, w_up, w_down, taps,
     out,
     beta_s, cum_s, keep_s, qd1, qd2, loc1, loc2, add1, add2, vf, gf, r1, r2, o1, o2,
-    pays, row_pays, heads, arrived, emit_w, skip, normed, wall, wdt, wd_own,
+    pay_a, pay_b, row_a, row_b, heads, arrived, emit_w, skip, normed, wall, wdt, wd_own,
     q1, k1, q2, k2, vals, gates, hidden,
     feat, low, hid, acc, d2d_out, d2d_in, far_out, msg_r, msg_l, far_in, in_l, in_r,
     load_sem, send_sem, recv_sem, wsend, wrecv,
@@ -233,54 +235,52 @@
 
     for c in loads[4:]:
         c.wait()
+    pays, row_pays = (pay_a, pay_b), (row_a, row_b)
     vf[...] = vals[...].astype(F32)
     gf[...] = gates[...].astype(F32)
     for h in range(2):
-        beta, cum = gate_rows(upd[...].astype(F32)[h : h + 1], fade[h], boost[h], level[0, h], bias[0, h])
+        beta, cum = gate_rows(
+            upd[...].astype(F32)[h : h + 1], fade[h], boost[h], level[0, h], bias[0, h]
+        )
         beta_s[h * NBLK : (h + 1) * NBLK, :] = beta
         cum_s[h * NBLK : (h + 1) * NBLK, :] = cum
 
-    def parts(it, carry):
-        todo = [(h, 2 * it + j) for j in range(2) for h in range(2)]
-        ins = []
-        for h, n in todo:
-            rows = pl.ds(pl.multiple_of(n * BLK, BLK), BLK)
-            if h == 0:
-                q, k = q1[rows, :].astype(F32), k1[rows, :].astype(F32)
-            else:
-                q, k = q2[:, rows].astype(F32).T, k2[:, rows].astype(F32).T
-            ins.append(
-                block_inputs(
-                    q,
-                    k,
-                    vf[pl.ds(2 * n * BLK + h, BLK, 2), :],
-                    cum_s[pl.ds(h * NBLK + n, 1), :],
-                    beta_s[pl.ds(h * NBLK + n, 1), :],
+    kept = ((qd1, loc1, add1, r1, o1), (qd2, loc2, add2, r2, o2))
+    sizes = (128, 64)
+
+    def parts_of(h):
+        qd, loc, add = kept[h][:3]
+
+        def parts(it, carry):
+            todo = [4 * it + j for j in range(4)]
+            ins = []
+            for n in todo:
+                rows = pl.ds(pl.multiple_of(n * BLK, BLK), BLK)
+                if h == 0:
+                    q, k = q1[rows, :].astype(F32), k1[rows, :].astype(F32)
+                else:
+                    q, k = q2[:, rows].astype(F32).T, k2[:, rows].astype(F32).T
+                ins.append(
+                    block_inputs(
+                        q,
+                        k,
+                        vf[pl.ds(2 * n * BLK + h, BLK, 2), :],
+                        cum_s[pl.ds(h * NBLK + n, 1), :],
+                        beta_s[pl.ds(h * NBLK + n, 1), :],
+                    )
                 )
-            )
-        extra = inverses([i["lower"] for i in ins])
-        for (h, n), i, e in zip(todo, ins, extra):
-            dk = (128, 64)[h]
-            solved = (i["right"] + mm(e, i["right"])).astype(BF16)
-            made = mm(jnp.concatenate([i["intra"], i["tail"]], axis=0), solved)
-            qd, loc, add = ((qd1, loc1, add1), (qd2, loc2, add2))[h]
-            qd[n, :BLK, :] = (i["query"] - made[:BLK, BLK:]).astype(BF16)
-            qd[n, BLK:, :] = (-made[BLK:, BLK:]).astype(BF16)
-            loc[n] = made[:BLK, :BLK]
-            add[n] = made[BLK:, :BLK]
-            keep_s[pl.ds(h * NBLK + n, 1), :] = i["keep"]
-        return carry
-
-    lax.fori_loop(0, 3, parts, 0)
-    for kind in range(2):
-        first_ring(0, kind, 0).wait_recv()
-        first_ring(0, kind, 2).start()
-        second_ring(0, kind, 0, 0).start()
-        second_ring(0, kind, 0, 1).start()
-    lax.fori_loop(3, NBLK // 2, parts, 0)
-    for kind in range(2):
-        first_ring(1, kind, 0).wait_recv()
-        first_ring(1, kind, 2).start()
+            extra = inverses([i["lower"] for i in ins])
+            for n, i, e in zip(todo, ins, extra):
+                solved = (i["right"] + mm(e, i["right"])).astype(BF16)
+                made = mm(jnp.concatenate([i["intra"], i["tail"]], axis=0), solved)
+                qd[n, :BLK, :] = (i["query"] - made[:BLK, BLK:]).astype(BF16)
+                qd[n, BLK:, :] = (-made[BLK:, BLK:]).astype(BF16)
+                loc[n] = made[:BLK, :BLK]
+                add[n] = made[BLK:, :BLK]
+                keep_s[pl.ds(h * NBLK + n, 1), :] = i["keep"]
+            return carry
+
+        return parts
 
     def eye(dk):
         return (
@@ -288,13 +288,13 @@
             == lax.broadcasted_iota(jnp.int32, (dk, dk), 1)
         ).astype(F32)
 
-    def chain(n, carry):
-        rows = pl.ds(pl.multiple_of(n * BLK, BLK), BLK)
-        out = []
-        for h, (state, total) in enumerate(carry):
-            dk = (128, 64)[h]
-            qd, loc, add = ((qd1, loc1, add1), (qd2, loc2, add2))[h]
-            r, o = ((r1, o1), (r2, o2))[h]
+    def local_map(h):
+        dk = sizes[h]
+        qd, loc, add, r, o = kept[h]
+
+        def chain(n, carry):
+            state, total = carry
+            rows = pl.ds(pl.multiple_of(n * BLK, BLK), BLK)
             made = mm(qd[n], state)
             o[rows, :] = loc[n] + made[:BLK, :BLK]
             r[rows, :] = made[:BLK, BLK:].astype(BF16)
@@ -302,151 +302,149 @@
             moved = made[BLK:]
             new_a = state[:, :BLK] * keep + moved[:, :BLK] + add[n]
             new_p = state[:, BLK:] * keep[:, :dk] + moved[:, BLK:]
-            out.append((jnp.concatenate([new_a, new_p], axis=1), total * keep))
-        return tuple(out)
-
-    start = tuple(
-        (jnp.concatenate([jnp.zeros((dk, BLK), F32), eye(dk)], axis=1), jnp.ones((1, BLK), F32))
-        for dk in (128, 64)
-    )
-    (s1, g1), (s2, g2) = lax.fori_loop(0, NBLK, chain, start)
-    write_maps(
-        pays,
-        y,
-        (s1[:, BLK:] - eye(128) * g1, s1[:, :BLK], g1[:, :1]),
-        (s2[:, BLK:] - eye(64) * g2[:, :64], s2[:, :BLK], g2[:, :1]),
-    )
-
-    def exchange(buf, dim, what):
-        sems = (send_sem, recv_sem)
-        return ring_copy(sems, 22 + dim * 3 + what, what, lambda i: buf.at[i], dim)
-
-    exchange(pays, 0, 0).start()
-    exchange(pays, 0, 1).start()
-    first_ring(0, 0, 1).wait_recv()
-    first_ring(0, 0, 2).wait_recv()
-    for piece in (1,):
-        second_ring(0, 0, piece, 0).start()
-        second_ring(0, 0, piece, 1).start()
-    exchange(pays, 0, 0).wait_recv()
-    exchange(pays, 0, 2).start()
-    for piece in (0,):
-        second_ring(0, 0, piece, 0).wait_recv()
-        second_ring(0, 0, piece, 2).start()
-    for piece in (0,):
-        second_ring(0, 1, piece, 0).wait_recv()
-        second_ring(0, 1, piece, 2).start()
-    exchange(pays, 0, 1).wait_recv()
-    exchange(pays, 0, 2).wait_recv()
-    whole = read_maps(pays, 0)
-    whole = tuple((d.astype(F32), a, g) for d, a, g in whole)
-    for i in range(1, 4):
-        whole = tuple(after(e, l) for e, l in zip(whole, read_maps(pays, i)))
-    write_maps(row_pays, z, *whole)
-    exchange(row_pays, 1, 0).start()
-    exchange(row_pays, 1, 1).start()
-    first_ring(0, 1, 1).wait_recv()
-    first_ring(0, 1, 2).wait_recv()
-    for piece in (1, 2, 3):
-        second_ring(0, 1, piece, 0).start()
-        second_ring(0, 1, piece, 1).start()
-    exchange(row_pays, 1, 0).wait_recv()
-    exchange(row_pays, 1, 2).start()
-    for piece in (2, 3):
-        second_ring(0, 0, piece, 0).start()
-        second_ring(0, 0, piece, 1).start()
-    exchange(row_pays, 1, 1).wait_recv()
-    exchange(row_pays, 1, 2).wait_recv()
-
-    states = [jnp.zeros((128, BLK), F32), jnp.zeros((64, BLK), F32)]
-    for buf, limit in ((row_pays, z), (pays, y)):
-        for i in range(3):
-            moved = [
-                s * g + a + mm(d, s) for (d, a, g), s in zip(read_maps(buf, i), states)
-            ]
-            states = [jnp.where(i < limit, m, s) for m, s in zip(moved, states)]
-    states = [s.astype(BF16) for s in states]
+            return jnp.concatenate([new_a, new_p], axis=1), total * keep
+
+        start = jnp.concatenate([jnp.zeros((dk, BLK), F32), eye(dk)], axis=1)
+        state, total = lax.fori_loop(0, NBLK, chain, (start, jnp.ones((1, BLK), F32)))
+        whole = (state[:, BLK:] - eye(dk) * total[:, :dk], state[:, :BLK], total[:, :1])
+        write_map(h, pays[h], y, whole)
+
+    def exchange(h, dim, what):
+        buf = (pays, row_pays)[dim][h]
+        k = 22 + (h * 2 + dim) * 3 + what
+        return ring_copy((send_sem, recv_sem), k, what, lambda i: buf.at[i], dim)
+
+    def first_wait(chunk, kind):
+        first_ring(chunk, kind, 1).wait_recv()
+        first_ring(chunk, kind, 2).wait_recv()
+
+    def second_start(chunk, kind, pieces):
+        for piece in pieces:
+            second_ring(chunk, kind, piece, 0).start()
+            second_ring(chunk, kind, piece, 1).start()
+
+    def second_pass(chunk, kind, pieces):
+        for piece in pieces:
+            second_ring(chunk, kind, piece, 0).wait_recv()
+            second_ring(chunk, kind, piece, 2).start()
+
+    def row_total(h):
+        exchange(h, 0, 1).wait_recv()
+        exchange(h, 0, 2).wait_recv()
+        d, a, g = read_map(h, pays[h], 0)
+        whole = (d.astype(F32), a, g)
+        for i in range(1, 4):
+            whole = after(whole, read_map(h, pays[h], i))
+        write_map(h, row_pays[h], z, whole)
+        exchange(h, 1, 0).start()
+        exchange(h, 1, 1).start()
+
+    def incoming(h):
+        exchange(h, 1, 1).wait_recv()
+        exchange(h, 1, 2).wait_recv()
+        state = jnp.zeros((sizes[h], BLK), F32)
+        for buf, limit in ((row_pays[h], z), (pays[h], y)):
+            for i in range(3):
+                d, a, g = read_map(h, buf, i)
+                state = jnp.where(i < limit, state * g + a + mm(d, state), state)
+        return state.astype(BF16)
 
     order = (far, far + 1 - 2 * core, right, right + 1 - 2 * core, left, left + 1 - 2 * core, mate)
 
-    def finish(n):
+    def finish(h, n, state):
+        r, o = kept[h][3:]
         rows = pl.ds(pl.multiple_of(n * BLK, BLK), BLK)
-        for h in range(2):
-            o, r = ((o1, r1), (o2, r2))[h]
-            head = o[rows, :] + mm(r[rows, :], states[h])
-            scale = lax.rsqrt(jnp.mean(head * head, axis=-1, keepdims=True) + EPSILON)
-            g = gf[pl.ds(2 * n * BLK + h, BLK, 2), :]
-            made = head * scale * norm_coef[...] * (0.5 * g * (1.0 + jnp.tanh(0.5 * g)))
-            heads[n, :, h * BLK : (h + 1) * BLK] = made.astype(BF16)
-
-    def hand_out(k):
+        head = o[rows, :] + mm(r[rows, :], state)
+        scale = lax.rsqrt(jnp.mean(head * head, axis=-1, keepdims=True) + EPSILON)
+        g = gf[pl.ds(2 * n * BLK + h, BLK, 2), :]
+        made = head * scale * norm_coef[...] * (0.5 * g * (1.0 + jnp.tanh(0.5 * g)))
+        heads[h, n] = made.astype(BF16)
+
+    def hand_out(h, k):
         return pltpu.make_async_remote_copy(
-            src_ref=heads.at[order[k]], dst_ref=arrived.at[me],
-            send_sem=send_sem.at[28 + k], recv_sem=recv_sem.at[28 + k],
+            src_ref=heads.at[h, order[k]], dst_ref=arrived.at[h, me],
+            send_sem=send_sem.at[47 + h * 7 + k], recv_sem=recv_sem.at[47 + h * 7 + k],
             device_id={"tp": order[k]}, device_id_type=MESH,
         )
 
-    for piece in (1,):
-        second_ring(0, 0, piece, 0).wait_recv()
-        second_ring(0, 0, piece, 2).start()
-    for k in range(7):
-        finish(order[k])
-        hand_out(k).start()
-    finish(me)
-    arrived[me] = heads[me]
-    for piece in (1,):
-        second_ring(0, 1, piece, 0).wait_recv()
-        second_ring(0, 1, piece, 2).start()
+    def finish_all(h, state):
+        for k in range(7):
+            finish(h, order[k], state)
+            hand_out(h, k).start()
+        finish(h, me, state)
+        arrived[h, me] = heads[h, me]
+
+    def emit(h, pair):
+        rows = jnp.concatenate([arrived[h, 2 * pair + i] for i in range(2)], axis=1)
+        span = pl.ds(pl.multiple_of(pair * 256 + h * 1024, 256), 256)
+
+        def tile(j, carry):
+            cols = pl.ds(pl.multiple_of(j * 512, 512), 512)
+            skip[:, cols] += mm(rows, emit_w[span, cols])
+            return carry
+
+        lax.fori_loop(0, 4, tile, 0, unroll=2)
+
+    lax.fori_loop(0, 2, parts_of(0), 0)
+    local_map(0)
+    exchange(0, 0, 0).start()
+    exchange(0, 0, 1).start()
+    for kind in range(2):
+        first_ring(0, kind, 0).wait_recv()
+        first_ring(0, kind, 2).start()
+    second_start(0, 0, (0,))
+    lax.fori_loop(0, 2, parts_of(1), 0)
+    exchange(0, 0, 0).wait_recv()
+    exchange(0, 0, 2).start()
+    for kind in range(2):
+        first_ring(1, kind, 0).wait_recv()
+        first_ring(1, kind, 2).start()
+    local_map(1)
+    exchange(1, 0, 0).start()
+    exchange(1, 0, 1).start()
+    second_start(0, 1, (0,))
+    row_total(0)
+    first_wait(0, 0)
+    second_ring(0, 0, 1, 0).start()
+    exchange(1, 0, 0).wait_recv()
+    exchange(1, 0, 2).start()
+    first_wait(0, 1)
+    second_start(0, 1, (1, 2, 3))
+    exchange(0, 1, 0).wait_recv()
+    exchange(0, 1, 2).start()
+    row_total(1)
+    second_ring(0, 0, 1, 1).start()
+    state_a = incoming(0)
+    exchange(1, 1, 0).wait_recv()
+    exchange(1, 1, 2).start()
+    second_pass(0, 0, (0,))
+    second_start(0, 0, (2, 3))
+    second_pass(0, 1, (0,))
+    finish_all(0, state_a)
+    second_pass(0, 0, (1,))
+    state_b = incoming(1)
+    finish_all(1, state_b)
+    second_pass(0, 1, (1,))
     skip[...] = hidden[...].astype(F32)
     loads[3].wait()
-
-    def emit(pair):
-        firsts = [arrived[2 * pair + i] for i in range(2)]
-        one = jnp.concatenate([f[:, :BLK] for f in firsts], axis=1)
-        two = jnp.concatenate([f[:, BLK:] for f in firsts], axis=1)
-        upper = pl.ds(pl.multiple_of(pair * 256, 256), 256)
-        lower = pl.ds(pl.multiple_of(pair * 256 + 1024, 256), 256)
-
-        def tile(j, carry):
-            cols = pl.ds(pl.multiple_of(j * 512, 512), 512)
-            skip[:, cols] += mm(one, emit_w[upper, cols]) + mm(two, emit_w[lower, cols])
-            return carry
-
-        lax.fori_loop(0, 4, tile, 0, unroll=2)
-
-    hand_out(6).wait_recv()
-    emit(x)
-    for piece in (2,):
-        second_ring(0, 1, piece, 0).wait_recv()
-        second_ring(0, 1, piece, 2).start()
-    for piece in (2,):
-        second_ring(0, 0, piece, 0).wait_recv()
-        second_ring(0, 0, piece, 2).start()
-    hand_out(2).wait_recv()
-    hand_out(3).wait_recv()
-    emit((x + 3) % 4)
-    for piece in (3,):
-        second_ring(0, 1, piece, 0).wait_recv()
-        second_ring(0, 1, piece, 2).start()
-    for piece in (3,):
-        second_ring(0, 0, piece, 0).wait_recv()
-        second_ring(0, 0, piece, 2).start()
-    hand_out(4).wait_recv()
-    hand_out(5).wait_recv()
-    emit((x + 1) % 4)
-    first_ring(1, 0, 1).wait_recv()
-    first_ring(1, 0, 2).wait_recv()
-    first_ring(1, 1, 1).wait_recv()
-    first_ring(1, 1, 2).wait_recv()
-    for piece in range(4):
-        second_ring(1, 0, piece, 0).start()
-        second_ring(1, 0, piece, 1).start()
-    for piece in range(4):
-        second_ring(1, 1, piece, 0).start()
-        second_ring(1, 1, piece, 1).start()
-    hand_out(0).wait_recv()
-    hand_out(1).wait_recv()
-    emit((x + 2) % 4)
+    hand_out(0, 6).wait_recv()
+    emit(0, x)
+    for h in range(2):
+        if h == 1:
+            hand_out(1, 6).wait_recv()
+            emit(1, x)
+        hand_out(h, 2).wait_recv()
+        hand_out(h, 3).wait_recv()
+        emit(h, (x + 3) % 4)
+        if h == 0:
+            second_pass(0, 1, (2,))
+        hand_out(h, 4).wait_recv()
+        hand_out(h, 5).wait_recv()
+        emit(h, (x + 1) % 4)
+        second_pass(0, h, (2 + h,))
+        hand_out(h, 0).wait_recv()
+        hand_out(h, 1).wait_recv()
+        emit(h, (x + 2) % 4)
     full = skip[...]
     norm = lax.rsqrt(jnp.mean(full * full, axis=-1, keepdims=True) + EPSILON)
     normed[...] = (full * norm * chan_coef[...]).astype(BF16)
@@ -472,6 +470,11 @@
     for c in own:
         c.start()
     a_right, b_left, b_right, a_left = tuple(own)
+    second_pass(0, 0, (3,))
+    for kind in range(2):
+        first_wait(1, kind)
+    second_start(1, 1, range(4))
+    second_start(1, 0, range(2))
     fwd_a = send(5, shard(left, 0, 64), shard(left, 0, 64), to_right)
     fwd_b = send(6, shard(right, 64, 64), shard(right, 64, 64), to_left)
     mate_la = send(7, shard(left, 0, 64), shard(left, 0, 64), to_mate)
@@ -520,21 +523,25 @@
 
     wide = (slice(0, 1024), slice(1024, 2048))
 
+    offsets = [(a, b) for a in (0, 1, 3) for b in (0, 1, 3)]
+    offsets += [(a, b) for a in range(4) for b in range(4) if a == 2 or b == 2]
+    columns = [((z + a) % 4) * 4 + (y + b) % 4 for a, b in offsets]
+
     def down(k, pair, sem, first=0, count=128, part=None):
         mine = pl.ds(pl.multiple_of(pair * 256 + core * 128 + first, 64), count)
         other = pl.ds(pl.multiple_of(pair * 256 + (1 - core) * 128 + first, 64), count)
         kept = slice(first, first + count)
 
-        def tile(j, carry):
-            span = pl.ds(pl.multiple_of(j * 256, 256), 256)
-            both = jnp.concatenate([hid[mine, :], hid[other, :]], axis=0)
-            made = mm(both, jnp.concatenate([wdt[2 * j], wdt[2 * j + 1]], axis=1))
+        tiles, cols = (range(8), slice(None))
+        if part is not None:
+            tiles, cols = (range(4 * part, 4 * part + 4), wide[part])
+        both = jnp.concatenate([hid[mine, :], hid[other, :]], axis=0)
+        for j in tiles:
+            span = slice(256 * j, 256 * j + 256)
+            weights = [wdt[columns[2 * j + i]] for i in range(2)]
+            made = mm(both, jnp.concatenate(weights, axis=1))
             acc[k, kept, span] = made[:count]
             d2d_out[k, kept, span] = made[count:].astype(BF16)
-            return carry
-
-        tiles, cols = ((0, 8), slice(None)) if part is None else ((4 * part, 4 * part + 4), wide[part])
-        lax.fori_loop(*tiles, tile, 0, unroll=4)
         sent = send(sem, d2d_out.at[k, kept, cols], d2d_in.at[k, kept, cols], to_mate)
         sent.start()
         return sent
@@ -575,6 +582,7 @@
         for piece in (1, 2, 3):
             second_ring(0, kind, piece, 1).wait_recv()
             second_ring(0, kind, piece, 2).wait_recv()
+    second_start(1, 0, (2, 3))
     own_mate.wait_recv()
     gate_up([x * 256])
 
@@ -591,11 +599,11 @@
     mate_la.wait_recv()
     mate_rb.wait_recv()
     early = [pair_l * 256, pair_l * 256 + 128, pair_r * 256 + 64, pair_r * 256 + 192]
+    gate_up(early, 0, 4)
     for kind in range(2):
         for piece in range(4):
             second_ring(1, kind, piece, 0).wait_recv()
             second_ring(1, kind, piece, 2).start()
-    gate_up(early, 0, 4)
     b_right.wait_recv()
     mate_lb.start()
     a_left.wait_recv()
@@ -620,29 +628,35 @@
     conv(pair_r, 0, 256)
     conv(pair_l, 64, 64)
     conv(pair_l, 192, 64)
+    for kind in range(2):
+        for piece in range(4):
+            second_ring(1, kind, piece, 1).wait_recv()
+    d_right = [down(1, pair_r, 12, part=0)]
+    d_left_b = [down(2, pair_l, 13, 64, 64, part=0)]
     fwd_a.wait_recv()
     mate_fa.start()
     fwd_b.wait_recv()
     mate_fb.start()
-    for kind in range(2):
-        for piece in range(4):
-            second_ring(1, kind, piece, 1).wait_recv()
-            second_ring(1, kind, piece, 2).wait_recv()
-    d_right, d_left_b = [], []
-    for c in range(2):
-        d_right.append(down(1, pair_r, (12, 43)[c], part=c))
-        d_left_b.append(down(2, pair_l, (13, 44)[c], 64, 64, part=c))
-    mate_fa.wait_recv()
-    mate_fb.wait_recv()
-    for c in range(2):
-        gate_up([pair_f * 256], 2 * c, 2 * c + 2)
+
+    def send_early(c):
         d_right[c].wait_recv()
         msg_r[top, wide[c]] = pair_sum(1, top, wide[c]).astype(BF16)
         r_a[c].start()
         d_left_b[c].wait_recv()
         msg_l[bottom, wide[c]] = pair_sum(2, bottom, wide[c]).astype(BF16)
         l_b[c].start()
+
+    send_early(0)
+    mate_fa.wait_recv()
+    mate_fb.wait_recv()
+    gate_up([pair_f * 256], 0, 4)
+    for kind in range(2):
+        for piece in range(4):
+            second_ring(1, kind, piece, 2).wait_recv()
+    d_right.append(down(1, pair_r, 43, part=1))
+    d_left_b.append(down(2, pair_l, 44, 64, 64, part=1))
     gate_up([pair_f * 256], 4, 6)
+    send_early(1)
 
     @pl.when(x == 1)
     def _():
@@ -691,17 +705,19 @@
         ).astype(BF16)
         r_b[c].start()
     d_own.wait_recv()
-    acc[3] = acc[3] + d2d_in[3].astype(F32) + skip[...]
+    acc[3] = acc[3] + d2d_in[3].astype(F32)
     for c in (*r_a, *l_b):
         c.wait_recv()
     acc[3, top, :] = acc[3, top, :] + in_l[top, :].astype(F32)
     acc[3, bottom, :] = acc[3, bottom, :] + in_r[bottom, :].astype(F32)
     for c in range(2):
-        cols = wide[c]
-        l_a[c].wait_recv()
-        out[top, cols] = (acc[3, top, cols] + in_r[top, cols].astype(F32)).astype(BF16)
-        r_b[c].wait_recv()
-        out[bottom, cols] = (acc[3, bottom, cols] + in_l[bottom, cols].astype(F32)).astype(BF16)
+        for rows, last, came in ((top, l_a, in_r), (bottom, r_b, in_l)):
+            last[c].wait_recv()
+            for i in range(8 * c, 8 * c + 8):
+                slot = slice(i * BLK, (i + 1) * BLK)
+                place_cols = pl.ds(pl.multiple_of(columns[i] * BLK, BLK), BLK)
+                total = acc[3, rows, slot] + came[rows, slot].astype(F32)
+                out[rows, place_cols] = (total + skip[rows, place_cols]).astype(BF16)
 
     for c in (own_mate, *own, fwd_a, fwd_b, mate_la, mate_lb, mate_ra, mate_rb, mate_fa, mate_fb):
         c.wait_send()
@@ -709,11 +725,12 @@
         c.wait_send()
     for c in (*r_a, *r_b, *l_a, *l_b):
         c.wait_send()
-    for dim, buf in ((0, pays), (1, row_pays)):
+    for h in range(2):
         for what in range(3):
-            exchange(buf, dim, what).wait_send()
-    for k in range(7):
-        hand_out(k).wait_send()
+            exchange(h, 0, what).wait_send()
+            exchange(h, 1, what).wait_send()
+        for k in range(7):
+            hand_out(h, k).wait_send()
     for chunk in range(2):
         for kind in range(2):
             for what in range(3):
@@ -746,10 +763,9 @@
             pltpu.VMEM((1024, 64), BF16),
             pltpu.VMEM((1024, BLK), F32),
             pltpu.VMEM((1024, BLK), F32),
-            pltpu.VMEM((4, 384, 128), BF16),
-            pltpu.VMEM((4, 384, 128), BF16),
-            pltpu.VMEM((8, 128, 256), BF16),
-            pltpu.VMEM((8, 128, 256), BF16),
+            *[pltpu.VMEM((4, 272, 128), BF16), pltpu.VMEM((4, 128, 128), BF16)] * 2,
+            pltpu.VMEM((2, 8, 128, 128), BF16),
+            pltpu.VMEM((2, 8, 128, 128), BF16),
             pltpu.VMEM((WIDTH, WIDTH), BF16),
             pltpu.VMEM((128, WIDTH), F32),
             pltpu.VMEM((128, WIDTH), BF16),
@@ -768,8 +784,8 @@
             pltpu.VMEM((4, 128, WIDTH), BF16),
             *[pltpu.VMEM(b, BF16) for b in block],
             pltpu.SemaphoreType.DMA((11,)),
-            pltpu.SemaphoreType.DMA((47,)),
-            pltpu.SemaphoreType.DMA((47,)),
+            pltpu.SemaphoreType.DMA((61,)),
+            pltpu.SemaphoreType.DMA((61,)),
             pltpu.SemaphoreType.DMA((60,)),
             pltpu.SemaphoreType.DMA((60,)),
         ],

time: 94.6 us -> 93.1 us (0.984)
  Pallas kernels: 92.5 us -> 91 us
    pallas_call x1, Pallas kernels: 92.5 us -> 91 us  [whole_layer(): pl.pallas_call(layer_kernel, out_shape=jax.ShapeDtypeStruct((128, WIDTH),...]
where the time goes in v4:
time: 93.1 us; the launch traced here: 92.9 us
  Pallas kernels  91 us (98%)
  local copies, waits for them, and re-layouts  1.88 us (2%)
    pallas_call x1, Pallas kernels, whole_layer(): pl.pallas_call(layer_kernel, out_shape=jax.ShapeDtypeStruct((128, WIDTH),...  91 us
    unnamed x1, local copies, waits for them, and re-layouts  1.88 us

profile of v4, /device:TPU:1, one launch (start us, length us, event | category | flops | bytes accessed | tf_op | source)
XLA Modules:
  0.0 92.9 jit_solution(8469446608337994295)
XLA Ops:
  0.0 91.0 %shard_map.181 = bf16[128,2048]{1,0:T(8,128)(2,1)} custom-call(bf16[1024,128]{1,0:T(8,128)(2,1)} %q1_in.1, bf16[1024,128]{1,0:T(8,128)(2,1)} %k1_in.1, bf16[64,1024]{1,0:T(8,128)(2,1)} %bitcast.11, bf16[64,1024]{1,0:T(8,128)(2,1)} %bitcast.12, bf16[2048,128]{1,0:T(8,128)(2,1)} %bitcast.9, bf16[2048,128]{1,0:T(8,128)(2,1)} %bitcast.10, ...), custom_call_target="tpu_custom_call" | custom-call | tf_op jit(solution)/shard_map/pallas_call | solution.py:747
  91.0 1.9 %copy.21 = bf16[128,2048]{1,0:T(8,128)(2,1)} copy(bf16[128,2048]{1,0:T(8,128)(2,1)} %shard_map.181) | data formatting | bytes 1048576
